TPU v7x, 512 devices: a whole 4x8x8 slice. The times are simulated.
512 devices in a mesh: sp: 64 (over z, y), tp: 8 (over x, core).
Axes of the slice: x: 4, y: 8, z: 8, core: 2. Of those that a mesh axis runs over, the one named last changes fastest.
Arguments:
- tokens: bfloat16 [24576, 2048], P('sp', 'tp'), may hold values from -40 to 40
- mix_gain: float32 [2048], replicated, may hold values from 0.1 to 1.9
- w_pool_in: bfloat16 [2048, 1024], P(None, 'tp'), may hold values from -0.125 to 0.125
- w_qlat: bfloat16 [2048, 512], P(None, 'tp'), may hold values from -0.125 to 0.125
- w_kvlat: bfloat16 [2048, 512], P(None, 'tp'), may hold values from -0.125 to 0.125
- w_krope: bfloat16 [2048, 64], replicated, may hold values from -0.125 to 0.125
- q_gain: float32 [512], replicated, may hold values from 1 to 60
- kv_gain: float32 [512], replicated, may hold values from 0.1 to 1.9
- w_q_content: bfloat16 [512, 2048], P(None, 'tp'), may hold values from -0.25 to 0.25
- w_q_rotary: bfloat16 [512, 1024], P(None, 'tp'), may hold values from -0.25 to 0.25
- w_key: bfloat16 [512, 2048], P(None, 'tp'), may hold values from -0.25 to 0.25
- w_value: bfloat16 [512, 2048], P(None, 'tp'), may hold values from -0.25 to 0.25
- pool_mix: bfloat16 [8, 128, 128], replicated, may hold values from -0.5 to 0.5
- pool_scale: float32 [1024], replicated, may hold values from 0.1 to 1.9
- w_out_pool: bfloat16 [1024, 2048], P('tp'), may hold values from -0.109375 to 0.109375
- w_out_attn: bfloat16 [2048, 2048], P('tp'), may hold values from -0.25 to 0.25
Outputs:
- layer_out: bfloat16 [24576, 2048], P(('sp', 'tp'))
- log_total: float32 [24576, 16], P('sp', 'tp')
All inputs are finite; a program needn't handle non-finite values.
Results may differ from a plain program's by a relative error of at most 0.015.
The roundings to bfloat16 on the way count: a program that leaves them out, or rounds other values in their place, can miss the bound.
Values may be sent and summed in bfloat16 or wider, within the bound.
A program may use at most 64 MiB of HBM per device.

v0:
```python
import jax
import jax.numpy as jnp
from jax import lax
from jax.sharding import PartitionSpec as P

NOPE = 128
ROPE = 64
VDIM = 128
GROUP_DIM = 128
WIDEST = 16
SPAN = 16


eps_norm = 1e-06
rope_base = 10000.0
masked_score = -1e30


def copy_for_each(x, axis):
    peers = lax.axis_size(axis)
    return lax.all_to_all(jnp.broadcast_to(x[None], (peers, *x.shape)), axis, 0, 0, tiled=True)


def joined_along(blocks, dim):
    lengths = list(blocks.shape[1:])
    lengths[dim] *= blocks.shape[0]
    return jnp.moveaxis(blocks, 0, dim).reshape(lengths)


def collect(x, axis, dim):
    blocks = copy_for_each(x, axis)
    return joined_along(blocks, dim)


def shortened(x):
    return jax.tree.map(lambda a: a.astype(jnp.bfloat16) if a.dtype == jnp.float32 else a, x)


def shifted(value, axis, steps):
    count = lax.axis_size(axis)
    leading, last = (max(0, -steps), min(count, count - steps))
    return lax.ppermute(value, axis, [(source, source + steps) for source in range(leading, last)])


def split_up(x, dim, peers):
    before, after = (x.shape[:dim], x.shape[dim + 1 :])
    return jnp.moveaxis(x.reshape(*before, peers, -1, *after), dim, 0)


def summed_on_arrival(x, axis, dim):
    peers = lax.axis_size(axis)
    blocks = lax.all_to_all(split_up(x, dim, peers), axis, 0, 0, tiled=True)
    return jnp.sum(blocks.astype(jnp.float32), axis=0)


def tables(positions, rotary_width):
    half_width = rotary_width // 2
    frequency = rope_base ** (-jnp.arange(half_width, dtype=jnp.float32) * 2.0 / rotary_width)
    angles = positions.astype(jnp.float32)[:, None] * frequency[None, :]
    return (jnp.cos(angles), jnp.sin(angles))


def rotate(vectors, cosine, sine_table):
    half_width = vectors.shape[-1] // 2
    first_half = vectors[..., :half_width]
    second_half = vectors[..., half_width:]
    return jnp.concatenate(
        [
            first_half * cosine - second_half * sine_table,
            second_half * cosine + first_half * sine_table,
        ],
        axis=-1,
    )


def latent_norm(latent, gain_vector):
    latent_values = latent.astype(jnp.float32)
    inverse = lax.rsqrt(jnp.mean(latent_values * latent_values, axis=-1, keepdims=True) + eps_norm)
    return (latent_values * inverse * gain_vector).astype(jnp.bfloat16)


def attend(
    softmax_state,
    query_content,
    query_rotary,
    key_content,
    key_rotary,
    values,
    allowed,
    score_scale,
):
    maxima, totals, summed = softmax_state
    scores = jnp.einsum(
        "qhd,khd->qhk", query_content, key_content, preferred_element_type=jnp.float32
    )
    scores = scores + jnp.einsum(
        "qhr,kr->qhk", query_rotary, key_rotary, preferred_element_type=jnp.float32
    )
    scores = jnp.where(allowed, scores * score_scale, masked_score)
    new_maxima = jnp.maximum(maxima, jnp.max(scores, axis=-1))
    factor = jnp.exp(maxima - new_maxima)
    expo = jnp.exp(scores - new_maxima[..., None])
    totals = totals * factor + jnp.sum(expo, axis=-1)
    summed = summed * factor[..., None] + jnp.einsum(
        "qhk,khd->qhd", expo.astype(jnp.bfloat16), values, preferred_element_type=jnp.float32
    )
    return (new_maxima, totals, summed)


def finish(softmax_state):
    maxima, totals, summed = softmax_state
    attended = (summed / totals[..., None]).astype(jnp.bfloat16)
    attended = attended.reshape(attended.shape[:-2] + (attended.shape[-2] * attended.shape[-1],))
    return (attended, maxima + jnp.log(totals))


def per_device(
    tokens,
    mix_gain,
    w_pool_in,
    w_qlat,
    w_kvlat,
    w_krope,
    q_gain,
    kv_gain,
    w_q_content,
    w_q_rotary,
    w_key,
    w_value,
    pool_mix,
    pool_scale,
    w_out_pool,
    w_out_attn,
):
    tp_size = lax.axis_size("tp")
    tp_rank = lax.axis_index("tp")
    sp_rank = lax.axis_index("sp")
    seq_count = lax.axis_size("sp") // SPAN
    local_rows, own_width = tokens.shape
    model_width = own_width * tp_size
    seq_rank = sp_rank // seq_count
    pool_cols = w_pool_in.shape[1]
    query_cols = w_qlat.shape[1]
    latent_cols = w_kvlat.shape[1]
    weight_cat = jnp.concatenate([w_pool_in, w_qlat, w_kvlat, w_krope], axis=1)
    raw_values = tokens.astype(jnp.float32)
    own_gain = lax.dynamic_slice_in_dim(mix_gain, tp_rank * own_width, own_width)
    squares = lax.psum(jnp.sum(raw_values * raw_values, axis=1), "tp")
    scaled = (raw_values * own_gain).astype(jnp.bfloat16)
    projected = jnp.dot(collect(scaled, "tp", 1), weight_cat, preferred_element_type=jnp.float32)
    inverse_rms = lax.rsqrt(squares / model_width + eps_norm)
    projected = (projected * inverse_rms[:, None]).astype(jnp.bfloat16)
    pool_pre = projected[:, :pool_cols]
    query_part = projected[:, pool_cols : pool_cols + query_cols]
    latent_part = projected[:, pool_cols + query_cols : pool_cols + query_cols + latent_cols]
    rotary_raw = projected[:, pool_cols + query_cols + latent_cols :]
    query_latent, kv_latent = (
        lax.all_gather(query_part, "tp", axis=1, tiled=True),
        lax.all_gather(latent_part, "tp", axis=1, tiled=True),
    )
    positions = seq_rank * local_rows + jnp.arange(local_rows, dtype=jnp.int32)
    query_normed = latent_norm(query_latent, q_gain)
    key_normed = latent_norm(kv_latent, kv_gain)
    own_heads = w_key.shape[1] // NOPE
    cosine, sine_table = tables(positions, ROPE)
    query_content = (
        jnp.dot(query_normed, w_q_content, preferred_element_type=jnp.float32)
        .astype(jnp.bfloat16)
        .reshape(local_rows, own_heads, NOPE)
    )
    key_content = (
        jnp.dot(key_normed, w_key, preferred_element_type=jnp.float32)
        .astype(jnp.bfloat16)
        .reshape(local_rows, own_heads, NOPE)
    )
    values = (
        jnp.dot(key_normed, w_value, preferred_element_type=jnp.float32)
        .astype(jnp.bfloat16)
        .reshape(local_rows, own_heads, VDIM)
    )
    query_rotary = rotate(
        jnp.dot(query_normed, w_q_rotary, preferred_element_type=jnp.float32).reshape(
            local_rows, own_heads, ROPE
        ),
        cosine[:, None, :],
        sine_table[:, None, :],
    ).astype(jnp.bfloat16)
    key_rotary = rotate(rotary_raw.astype(jnp.float32), cosine, sine_table).astype(jnp.bfloat16)
    score_scale = (NOPE + ROPE) ** (-0.5)
    local_index = jnp.arange(local_rows, dtype=jnp.int32)
    bit_count = SPAN.bit_length() - 1
    initial = (
        jnp.full((local_rows, own_heads), masked_score, jnp.float32),
        jnp.zeros((local_rows, own_heads), jnp.float32),
        jnp.zeros((local_rows, own_heads, VDIM), jnp.float32),
    )
    causal = local_index[None, None, :] <= local_index[:, None, None]
    softmax_state = attend(
        initial, query_content, query_rotary, key_content, key_rotary, values, causal, score_scale
    )
    earlier_blocks = (key_content[None], key_rotary[None], values[None])
    for doubling_level in range(bit_count):
        arrived = jax.tree.map(
            lambda part, own: part.astype(own.dtype),
            shifted(shortened(earlier_blocks), "sp", seq_count * 2**doubling_level),
            earlier_blocks,
        )
        earlier_blocks = tuple(
            (
                jnp.concatenate([earlier, later], axis=0)
                for earlier, later in zip(arrived, earlier_blocks)
            )
        )

    def visit_block(block_index, state_now):
        distance = SPAN - 1 - block_index
        return attend(
            state_now,
            query_content,
            query_rotary,
            earlier_blocks[0][block_index],
            earlier_blocks[1][block_index],
            earlier_blocks[2][block_index],
            seq_rank >= distance,
            score_scale,
        )

    softmax_state = lax.fori_loop(0, SPAN - 1, visit_block, softmax_state)
    attended, log_total = finish(softmax_state)
    group_count = pool_cols // GROUP_DIM
    rim_rows = shifted(pool_pre[local_rows - (WIDEST - 1) :], "sp", seq_count)
    rim_rows = jnp.where(seq_rank > 0, rim_rows, jnp.zeros_like(rim_rows))
    pool_values = pool_pre.astype(jnp.float32)
    extended = jnp.concatenate([rim_rows.astype(jnp.float32), pool_values], axis=0)
    groups = tp_rank * group_count + jnp.arange(pool_cols, dtype=jnp.int32) // GROUP_DIM
    windows = jnp.left_shift(jnp.int32(2), groups % 4)
    window_sums = jnp.zeros((local_rows, pool_cols), jnp.float32)
    for distance in range(WIDEST):
        window_sums = window_sums + jnp.where(
            distance < windows[None, :],
            extended[WIDEST - 1 - distance : WIDEST - 1 - distance + local_rows],
            0.0,
        )
    counts = jnp.minimum(positions[:, None] + 1, windows[None, :]).astype(jnp.float32)
    pooled = (window_sums / counts - pool_values).astype(jnp.bfloat16)
    own_mix = lax.dynamic_slice_in_dim(pool_mix, tp_rank * group_count, group_count, 0)
    mixed_pool = jnp.einsum(
        "rgc,gcd->rgd",
        pooled.reshape(local_rows, group_count, GROUP_DIM),
        own_mix,
        preferred_element_type=jnp.float32,
    ).reshape(local_rows, pool_cols)
    own_scale = lax.dynamic_slice_in_dim(pool_scale, tp_rank * pool_cols, pool_cols)
    pool_out = (mixed_pool * own_scale).astype(jnp.bfloat16)
    layer_out = summed_on_arrival(
        (
            jnp.dot(pool_out, w_out_pool, preferred_element_type=jnp.float32)
            + jnp.dot(attended, w_out_attn, preferred_element_type=jnp.float32)
        ).astype(jnp.bfloat16),
        "tp",
        0,
    )
    return (layer_out.astype(jnp.bfloat16), log_total)


def solution(mesh):
    in_specs = (
        P("sp", "tp"),
        P(),
        P(None, "tp"),
        P(None, "tp"),
        P(None, "tp"),
        P(),
        P(),
        P(),
        P(None, "tp"),
        P(None, "tp"),
        P(None, "tp"),
        P(None, "tp"),
        P(),
        P(),
        P("tp", None),
        P("tp", None),
    )
    out_specs = (P(("sp", "tp"), None), P("sp", "tp"))
    return jax.shard_map(
        per_device, mesh=mesh, in_specs=in_specs, out_specs=out_specs, check_vma=False
    )
```

profile of v0, /device:TPU:128, one launch (start us, length us, event | category | flops | bytes accessed | tf_op | source)
XLA Modules:
  0.0 444.7 jit_solution(10551901377013151352)
XLA Ops:
  4.1 4.4 all-to-all-start
  15.1 19.9 %psum.7 = f32[384]{0:T(512)S(1)} all-reduce(f32[384]{0:T(512)S(1)} %get-tuple-element.225), channel_id=1, replica_groups=mesh['sp'=64,'tp'=8] {'tp'}, use_global_device_ids=true, to_apply=%region_1.2 | all-reduce | flops 384 | bytes 3072 | tf_op jit(solution)/shard_map/psum | solution.py:148
  42.4 13.1 %all_gather.6 = bf16[384,512]{0,1:T(8,128)(2,1)S(1)} all-gather(bf16[384,64]{0,1:T(8,128)(2,1)S(1)} %get-tuple-element.224), channel_id=1, replica_groups=mesh['sp'=64,'tp'=8] {'tp'}, dimensions={1}, use_global_device_ids=true | all-gather | bytes 442368 | tf_op jit(solution)/shard_map/all_gather | solution.py:159
  56.1 7.9 %collective-permute-start.9 = (bf16[1,384,2,128]{1,3,2,0:T(8,128)(2,1)S(1)}, bf16[1,384,2,128]{1,3,2,0:T(8,128)(2,1)S(1)}, u32[]{:S(2)}, u32[]{:S(2)}) collective-permute-start(bf16[1,384,2,128]{1,3,2,0:T(8,128)(2,1)S(1)} %bitcast.93), channel_id=1, source_target_pairs={{0,32},{8,40},{16,48},{24,56},{32,64},{40,72},{48,80},{56,88},{64,... | collective-permute-start | bytes 589832 | tf_op jit(solution)/shard_map/ppermute | solution.py:42
  64.3 4.0 collective-permute-start.5
  68.9 7.8 %collective-permute-start.1 = (bf16[1,384,2,128]{3,1,2,0:T(8,128)(2,1)S(1)}, bf16[1,384,2,128]{3,1,2,0:T(8,128)(2,1)S(1)}, u32[]{:S(2)}, u32[]{:S(2)}) collective-permute-start(bf16[1,384,2,128]{3,1,2,0:T(8,128)(2,1)S(1)} %copy.39), channel_id=1, source_target_pairs={{0,32},{8,40},{16,48},{24,56},{32,64},{40,72},{48,80},{56,88},{64,... | collective-permute-start | bytes 589832 | tf_op jit(solution)/shard_map/ppermute | solution.py:42
  76.6 13.0 %all_gather.7 = bf16[384,512]{0,1:T(8,128)(2,1)S(1)} all-gather(bf16[384,64]{0,1:T(8,128)(2,1)S(1)} %get-tuple-element.223), channel_id=1, replica_groups=mesh['sp'=64,'tp'=8] {'tp'}, dimensions={1}, use_global_device_ids=true | all-gather | bytes 442368 | tf_op jit(solution)/shard_map/all_gather | solution.py:158
  91.3 5.5 %collective-permute-start.10 = (bf16[2,384,2,128]{1,3,2,0:T(8,128)(2,1)S(1)}, bf16[2,384,2,128]{1,3,2,0:T(8,128)(2,1)S(1)}, u32[]{:S(2)}, u32[]{:S(2)}) collective-permute-start(bf16[2,384,2,128]{1,3,2,0:T(8,128)(2,1)S(1)} %pad_maximum_fusion.5), channel_id=1, source_target_pairs={{0,64},{8,72},{16,80},{24,88},{32,96},{40,104},{48,112},{56,120},{... | collective-permute-start | bytes 1179656 | tf_op jit(solution)/shard_map/ppermute | solution.py:42
  100.6 5.6 %collective-permute-done.10 = bf16[2,384,2,128]{1,3,2,0:T(8,128)(2,1)S(1)} collective-permute-done((bf16[2,384,2,128]{1,3,2,0:T(8,128)(2,1)S(1)}, bf16[2,384,2,128]{1,3,2,0:T(8,128)(2,1)S(1)}, u32[]{:S(2)}, u32[]{:S(2)}) %collective-permute-start.10) | collective-permute-done | bytes 393248 | tf_op jit(solution)/shard_map/ppermute | solution.py:42
  106.3 6.5 %collective-permute-start.11 = (bf16[4,384,2,128]{1,3,2,0:T(8,128)(2,1)S(1)}, bf16[4,384,2,128]{1,3,2,0:T(8,128)(2,1)S(1)}, u32[]{:S(2)}, u32[]{:S(2)}) collective-permute-start(bf16[4,384,2,128]{1,3,2,0:T(8,128)(2,1)S(1)} %pad_maximum_fusion.3), channel_id=1, source_target_pairs={{0,128},{8,136},{16,144},{24,152},{32,160},{40,168},{48,176},{56,1... | collective-permute-start | bytes 2359304 | tf_op jit(solution)/shard_map/ppermute | solution.py:42
  115.3 15.2 %collective-permute-done.2 = bf16[2,384,2,128]{3,1,2,0:T(8,128)(2,1)S(1)} collective-permute-done((bf16[2,384,2,128]{3,1,2,0:T(8,128)(2,1)S(1)}, bf16[2,384,2,128]{3,1,2,0:T(8,128)(2,1)S(1)}, u32[]{:S(2)}, u32[]{:S(2)}) %collective-permute-start.2) | collective-permute-done | bytes 393248 | tf_op jit(solution)/shard_map/ppermute | solution.py:42
  130.5 5.4 %collective-permute-start.3 = (bf16[4,384,2,128]{3,1,2,0:T(8,128)(2,1)S(1)}, bf16[4,384,2,128]{3,1,2,0:T(8,128)(2,1)S(1)}, u32[]{:S(2)}, u32[]{:S(2)}) collective-permute-start(bf16[4,384,2,128]{3,1,2,0:T(8,128)(2,1)S(1)} %pad_maximum_fusion.2), channel_id=1, source_target_pairs={{0,128},{8,136},{16,144},{24,152},{32,160},{40,168},{48,176},{56,1... | collective-permute-start | bytes 2359304 | tf_op jit(solution)/shard_map/ppermute | solution.py:42
  136.0 30.4 %collective-permute-done.6 = bf16[2,384,64]{1,2,0:T(8,128)(2,1)S(1)} collective-permute-done((bf16[2,384,64]{1,2,0:T(8,128)(2,1)S(1)}, bf16[2,384,64]{1,2,0:T(8,128)(2,1)S(1)}, u32[]{:S(2)}, u32[]{:S(2)}) %collective-permute-start.6) | collective-permute-done | bytes 98336 | tf_op jit(solution)/shard_map/ppermute | solution.py:42
  166.3 5.3 %collective-permute-start.7 = (bf16[4,384,64]{1,2,0:T(8,128)(2,1)S(1)}, bf16[4,384,64]{1,2,0:T(8,128)(2,1)S(1)}, u32[]{:S(2)}, u32[]{:S(2)}) collective-permute-start(bf16[4,384,64]{1,2,0:T(8,128)(2,1)S(1)} %maximum_maximum_fusion.1), channel_id=1, source_target_pairs={{0,128},{8,136},{16,144},{24,152},{32,160},{40,168},{48,176},{56,1... | collective-permute-start | bytes 589832 | tf_op jit(solution)/shard_map/ppermute | solution.py:42
  173.2 4.2 collective-permute-start.12
  177.7 49.1 %collective-permute-done.7 = bf16[4,384,64]{1,2,0:T(8,128)(2,1)S(1)} collective-permute-done((bf16[4,384,64]{1,2,0:T(8,128)(2,1)S(1)}, bf16[4,384,64]{1,2,0:T(8,128)(2,1)S(1)}, u32[]{:S(2)}, u32[]{:S(2)}) %collective-permute-start.7) | collective-permute-done | bytes 196640 | tf_op jit(solution)/shard_map/ppermute | solution.py:42
  235.1 26.3 %collective-permute-start = (bf16[15,128]{0,1:T(8,128)(2,1)}, bf16[15,128]{0,1:T(8,128)(2,1)S(1)}, u32[]{:S(2)}, u32[]{:S(2)}) collective-permute-start(bf16[15,128]{0,1:T(8,128)(2,1)} %slice.98), channel_id=1, source_target_pairs={{0,32},{8,40},{16,48},{24,56},{32,64},{40,72},{48,80},{56,88},{64,... | collective-permute-start | bytes 11528 | tf_op jit(solution)/shard_map/ppermute | solution.py:42
  262.5 5.1 %collective-permute-done = bf16[15,128]{0,1:T(8,128)(2,1)S(1)} collective-permute-done((bf16[15,128]{0,1:T(8,128)(2,1)}, bf16[15,128]{0,1:T(8,128)(2,1)S(1)}, u32[]{:S(2)}, u32[]{:S(2)}) %collective-permute-start) | collective-permute-done | bytes 3872 | tf_op jit(solution)/shard_map/ppermute | solution.py:42
  268.3 44.2 %collective-permute-done.8 = bf16[8,384,64]{1,2,0:T(8,128)(2,1)} collective-permute-done((bf16[8,384,64]{1,2,0:T(8,128)(2,1)}, bf16[8,384,64]{1,2,0:T(8,128)(2,1)}, u32[]{:S(2)}, u32[]{:S(2)}) %collective-permute-start.8) | collective-permute-done | bytes 393248 | tf_op jit(solution)/shard_map/ppermute | solution.py:42
  317.6 27.7 %collective-permute-done.4 = bf16[8,384,2,128]{3,1,2,0:T(8,128)(2,1)} collective-permute-done((bf16[8,384,2,128]{3,1,2,0:T(8,128)(2,1)}, bf16[8,384,2,128]{3,1,2,0:T(8,128)(2,1)}, u32[]{:S(2)}, u32[]{:S(2)}) %collective-permute-start.4) | collective-permute-done | bytes 1572896 | tf_op jit(solution)/shard_map/ppermute | solution.py:42
  351.1 59.7 %while.17 = (s32[]{:T(128)}, f32[384,2]{0,1:T(2,128)S(1)}, f32[384,2]{0,1:T(2,128)S(1)}, f32[384,2,128]{0,2,1:T(8,128)S(1)}, s32[]{:T(128)}, /*index=5*/bf16[16,...) while((s32[]{:T(128)}, f32[384,2]{0,1:T(2,128)S(1)}, ...), condition=%wide.region_9.10_spmd, body=%wide.region_6.9_spmd.sunk | while | flops 191301120 | bytes 7472779 | solution.py:228
  413.5 5.2 %add_convert_fusion = bf16[384,2048]{1,0:T(8,128)(2,1)} fusion(f32[384,2048]{1,0:T(8,128)} %fusion.163, bf16[128,2048]{1,0:T(8,128)(2,1)S(1)} %copy-done.15, f32[384,128]{0,1:T(8,128)S(1)} %copy-done.13, f32[15,128]{0,1:T(8,128)S(1)} %copy-done.14, f32[128]{0:T(128)S(1)} %copy-done.23, s32[128]{0:T(128)S(1)} %copy-done.38, s32[384]{0:T(512)S(1)} %fusion.148, ...), kind=kOutput, calls=%fused_computation.22 | convolution fusion | flops 218087424 | bytes 5484548 | tf_op jit(solution)/shard_map/dot_general | solution.py:257
  418.7 3.6 all-to-all-start.1
  422.9 20.9 %all-to-all-done.1 = bf16[8,48,2048]{2,1,0:T(8,128)(2,1)S(1)} async-done(((bf16[8,48,2048]{2,1,0:T(8,128)(2,1)}), bf16[8,48,2048]{2,1,0:T(8,128)(2,1)S(1)}, u32[]{:S(2)}, u32[]{:S(2)}) %all-to-all-start.1) | async-done | bytes 1572896 | tf_op jit(solution)/shard_map/all_to_all | solution.py:52
  (269 shorter events, 112.3 us)
Async XLA Ops:
  0.6 410.3 %copy-start = (bf16[256,2048]{1,0:T(8,128)(2,1)S(1)}, bf16[256,2048]{1,0:T(8,128)(2,1)}, u32[]{:S(2)}) copy-start(bf16[256,2048]{1,0:T(8,128)(2,1)} %param.33) | copy-start | bytes 3145732
  4.1 35.6 %all-to-all-start = ((bf16[8,384,256]{1,2,0:T(8,128)(2,1)}), bf16[8,384,256]{1,2,0:T(8,128)(2,1)S(1)}, u32[]{:S(2)}, u32[]{:S(2)}) async-start(bf16[8,384,256]{1,2,0:T(8,128)(2,1)} %broadcast_in_dim.180), calls=%async_computation | async-start | bytes 3145728 | tf_op jit(solution)/shard_map/all_to_all | solution.py:21
  39.7 16.0 %copy-start.16 = (bf16[512,256]{1,0:T(8,128)(2,1)S(1)}, bf16[512,256]{1,0:T(8,128)(2,1)}, u32[]{:S(2)}) copy-start(bf16[512,256]{1,0:T(8,128)(2,1)} %param.29) | copy-start | bytes 786436
  42.4 26.3 %copy-start.10 = (bf16[384,320]{0,1:T(8,128)(2,1)}, bf16[384,320]{0,1:T(8,128)(2,1)S(1)}, u32[]{:S(2)}) copy-start(bf16[384,320]{0,1:T(8,128)(2,1)S(1)} %fusion.31) | copy-start | bytes 737284
  42.4 25.9 %copy-start.17 = (bf16[512,256]{1,0:T(8,128)(2,1)S(1)}, bf16[512,256]{1,0:T(8,128)(2,1)}, u32[]{:S(2)}) copy-start(bf16[512,256]{1,0:T(8,128)(2,1)} %param.28) | copy-start | bytes 786436
  56.1 33.6 %copy-start.19 = (bf16[512,128]{1,0:T(8,128)(2,1)S(1)}, bf16[512,128]{1,0:T(8,128)(2,1)}, u32[]{:S(2)}) copy-start(bf16[512,128]{1,0:T(8,128)(2,1)} %param.27) | copy-start | bytes 393220
  56.1 33.6 %copy-start.21 = (f32[512]{0:T(512)S(1)}, f32[512]{0:T(512)}, u32[]{:S(2)}) copy-start(f32[512]{0:T(512)} %param.24) | copy-start | bytes 6148
  56.1 34.8 %collective-permute-start.9 = (bf16[1,384,2,128]{1,3,2,0:T(8,128)(2,1)S(1)}, bf16[1,384,2,128]{1,3,2,0:T(8,128)(2,1)S(1)}, u32[]{:S(2)}, u32[]{:S(2)}) collective-permute-start(bf16[1,384,2,128]{1,3,2,0:T(8,128)(2,1)S(1)} %bitcast.93), channel_id=1, source_target_pairs={{0,32},{8,40},{16,48},{24,56},{32,64},{40,72},{48,80},{56,88},{64,... | collective-permute-start | bytes 589832 | tf_op jit(solution)/shard_map/ppermute | solution.py:42
  64.3 25.8 %copy-start.18 = (bf16[512,256]{1,0:T(8,128)(2,1)S(1)}, bf16[512,256]{1,0:T(8,128)(2,1)}, u32[]{:S(2)}) copy-start(bf16[512,256]{1,0:T(8,128)(2,1)} %param.26) | copy-start | bytes 786436
  64.3 48.8 %collective-permute-start.5 = (bf16[1,384,64]{1,2,0:T(8,128)(2,1)S(1)}, bf16[1,384,64]{1,2,0:T(8,128)(2,1)S(1)}, u32[]{:S(2)}, u32[]{:S(2)}) collective-permute-start(bf16[1,384,64]{1,2,0:T(8,128)(2,1)S(1)} %pad_maximum_fusion.8), channel_id=1, source_target_pairs={{0,32},{8,40},{16,48},{24,56},{32,64},{40,72},{48,80},{56,88},{64,... | collective-permute-start | bytes 147464 | tf_op jit(solution)/shard_map/ppermute | solution.py:42
  68.9 28.3 %collective-permute-start.1 = (bf16[1,384,2,128]{3,1,2,0:T(8,128)(2,1)S(1)}, bf16[1,384,2,128]{3,1,2,0:T(8,128)(2,1)S(1)}, u32[]{:S(2)}, u32[]{:S(2)}) collective-permute-start(bf16[1,384,2,128]{3,1,2,0:T(8,128)(2,1)S(1)} %copy.39), channel_id=1, source_target_pairs={{0,32},{8,40},{16,48},{24,56},{32,64},{40,72},{48,80},{56,88},{64,... | collective-permute-start | bytes 589832 | tf_op jit(solution)/shard_map/ppermute | solution.py:42
  91.3 15.0 %collective-permute-start.10 = (bf16[2,384,2,128]{1,3,2,0:T(8,128)(2,1)S(1)}, bf16[2,384,2,128]{1,3,2,0:T(8,128)(2,1)S(1)}, u32[]{:S(2)}, u32[]{:S(2)}) collective-permute-start(bf16[2,384,2,128]{1,3,2,0:T(8,128)(2,1)S(1)} %pad_maximum_fusion.5), channel_id=1, source_target_pairs={{0,64},{8,72},{16,80},{24,88},{32,96},{40,104},{48,112},{56,120},{... | collective-permute-start | bytes 1179656 | tf_op jit(solution)/shard_map/ppermute | solution.py:42
  97.2 33.2 %collective-permute-start.2 = (bf16[2,384,2,128]{3,1,2,0:T(8,128)(2,1)S(1)}, bf16[2,384,2,128]{3,1,2,0:T(8,128)(2,1)S(1)}, u32[]{:S(2)}, u32[]{:S(2)}) collective-permute-start(bf16[2,384,2,128]{3,1,2,0:T(8,128)(2,1)S(1)} %pad_maximum_fusion.4), channel_id=1, source_target_pairs={{0,64},{8,72},{16,80},{24,88},{32,96},{40,104},{48,112},{56,120},{... | collective-permute-start | bytes 1179656 | tf_op jit(solution)/shard_map/ppermute | solution.py:42
  106.3 65.4 %collective-permute-start.11 = (bf16[4,384,2,128]{1,3,2,0:T(8,128)(2,1)S(1)}, bf16[4,384,2,128]{1,3,2,0:T(8,128)(2,1)S(1)}, u32[]{:S(2)}, u32[]{:S(2)}) collective-permute-start(bf16[4,384,2,128]{1,3,2,0:T(8,128)(2,1)S(1)} %pad_maximum_fusion.3), channel_id=1, source_target_pairs={{0,128},{8,136},{16,144},{24,152},{32,160},{40,168},{48,176},{56,1... | collective-permute-start | bytes 2359304 | tf_op jit(solution)/shard_map/ppermute | solution.py:42
  113.1 53.2 %collective-permute-start.6 = (bf16[2,384,64]{1,2,0:T(8,128)(2,1)S(1)}, bf16[2,384,64]{1,2,0:T(8,128)(2,1)S(1)}, u32[]{:S(2)}, u32[]{:S(2)}) collective-permute-start(bf16[2,384,64]{1,2,0:T(8,128)(2,1)S(1)} %maximum_maximum_fusion.2), channel_id=1, source_target_pairs={{0,64},{8,72},{16,80},{24,88},{32,96},{40,104},{48,112},{56,120},{... | collective-permute-start | bytes 294920 | tf_op jit(solution)/shard_map/ppermute | solution.py:42
  130.5 99.3 %collective-permute-start.3 = (bf16[4,384,2,128]{3,1,2,0:T(8,128)(2,1)S(1)}, bf16[4,384,2,128]{3,1,2,0:T(8,128)(2,1)S(1)}, u32[]{:S(2)}, u32[]{:S(2)}) collective-permute-start(bf16[4,384,2,128]{3,1,2,0:T(8,128)(2,1)S(1)} %pad_maximum_fusion.2), channel_id=1, source_target_pairs={{0,128},{8,136},{16,144},{24,152},{32,160},{40,168},{48,176},{56,1... | collective-permute-start | bytes 2359304 | tf_op jit(solution)/shard_map/ppermute | solution.py:42
  166.3 60.4 %collective-permute-start.7 = (bf16[4,384,64]{1,2,0:T(8,128)(2,1)S(1)}, bf16[4,384,64]{1,2,0:T(8,128)(2,1)S(1)}, u32[]{:S(2)}, u32[]{:S(2)}) collective-permute-start(bf16[4,384,64]{1,2,0:T(8,128)(2,1)S(1)} %maximum_maximum_fusion.1), channel_id=1, source_target_pairs={{0,128},{8,136},{16,144},{24,152},{32,160},{40,168},{48,176},{56,1... | collective-permute-start | bytes 589832 | tf_op jit(solution)/shard_map/ppermute | solution.py:42
  173.2 142.4 %collective-permute-start.12 = (bf16[8,384,2,128]{1,3,2,0:T(8,128)(2,1)}, bf16[8,384,2,128]{1,3,2,0:T(8,128)(2,1)}, u32[]{:S(2)}, u32[]{:S(2)}) collective-permute-start(bf16[8,384,2,128]{1,3,2,0:T(8,128)(2,1)} %pad_maximum_fusion.1), channel_id=1, source_target_pairs={{0,256},{8,264},{16,272},{24,280},{32,288},{40,296},{48,304},{56,3... | collective-permute-start | bytes 4718600 | tf_op jit(solution)/shard_map/ppermute | solution.py:42
  227.6 84.9 %collective-permute-start.8 = (bf16[8,384,64]{1,2,0:T(8,128)(2,1)}, bf16[8,384,64]{1,2,0:T(8,128)(2,1)}, u32[]{:S(2)}, u32[]{:S(2)}) collective-permute-start(bf16[8,384,64]{1,2,0:T(8,128)(2,1)} %maximum_maximum_fusion), channel_id=1, source_target_pairs={{0,256},{8,264},{16,272},{24,280},{32,288},{40,296},{48,304},{56,3... | collective-permute-start | bytes 1179656 | tf_op jit(solution)/shard_map/ppermute | solution.py:42
  231.2 114.0 %collective-permute-start.4 = (bf16[8,384,2,128]{3,1,2,0:T(8,128)(2,1)}, bf16[8,384,2,128]{3,1,2,0:T(8,128)(2,1)}, u32[]{:S(2)}, u32[]{:S(2)}) collective-permute-start(bf16[8,384,2,128]{3,1,2,0:T(8,128)(2,1)} %pad_maximum_fusion), channel_id=1, source_target_pairs={{0,256},{8,264},{16,272},{24,280},{32,288},{40,296},{48,304},{56,3... | collective-permute-start | bytes 4718600 | tf_op jit(solution)/shard_map/ppermute | solution.py:42
  235.1 32.6 %collective-permute-start = (bf16[15,128]{0,1:T(8,128)(2,1)}, bf16[15,128]{0,1:T(8,128)(2,1)S(1)}, u32[]{:S(2)}, u32[]{:S(2)}) collective-permute-start(bf16[15,128]{0,1:T(8,128)(2,1)} %slice.98), channel_id=1, source_target_pairs={{0,32},{8,40},{16,48},{24,56},{32,64},{40,72},{48,80},{56,88},{64,... | collective-permute-start | bytes 11528 | tf_op jit(solution)/shard_map/ppermute | solution.py:42
  317.5 33.6 %copy-start.5 = (bf16[16,384,2,128]{1,3,2,0:T(8,128)(2,1)}, bf16[16,384,2,128]{1,3,2,0:T(8,128)(2,1)S(1)}, u32[]{:S(2)}) copy-start(bf16[16,384,2,128]{1,3,2,0:T(8,128)(2,1)S(1)} %constant_dynamic-update-slice_fusion.10) | copy-start | bytes 9437188
  317.5 30.4 %copy-start.4 = (bf16[4,384,2,128]{3,1,2,0:T(8,128)(2,1)S(1)}, bf16[4,384,2,128]{3,1,2,0:T(8,128)(2,1)}, u32[]{:S(2)}) copy-start(bf16[4,384,2,128]{3,1,2,0:T(8,128)(2,1)} %copy-done.3) | copy-start | bytes 2359300
  418.7 25.1 %all-to-all-start.1 = ((bf16[8,48,2048]{2,1,0:T(8,128)(2,1)}), bf16[8,48,2048]{2,1,0:T(8,128)(2,1)S(1)}, u32[]{:S(2)}, u32[]{:S(2)}) async-start(bf16[8,48,2048]{2,1,0:T(8,128)(2,1)} %bitcast.100), calls=%async_computation.1 | async-start | bytes 3145728 | tf_op jit(solution)/shard_map/all_to_all | solution.py:52
  (30 other events, 93.0 us)
where the time goes:
time: 447 us; the launch traced here: 445 us
  waiting for transfers between devices  198 us (44%)
  starting transfers between devices  91 us (20%)
  matrix products  68.6 us (15%)
  blocking collectives  46 us (10%)
  local copies, waits for them, and re-layouts  21 us (5%)
  other arithmetic  17.6 us (4%)
    ppermute x13, waiting for transfers between devices, shifted(): lax.ppermute(value, axis, [(source, source + steps) for source in range(l...  177 us
    ppermute x13, starting transfers between devices, shifted(): lax.ppermute(value, axis, [(source, source + steps) for source in range(l...  83 us
    all_to_all x1, waiting for transfers between devices, summed_on_arrival(): blocks = lax.all_to_all(split_up(x, dim, peers), axis, 0, 0, tiled=True)  20.9 us
    dot_general x16, matrix products, attend(): jnp.einsum('qhk,khd->qhd', expo.astype(jnp.bfloat16), values, preferred_e...  20.1 us
    psum x1, blocking collectives, per_device(): squares = lax.psum(jnp.sum(raw_values * raw_values, axis=1), 'tp')  19.9 us
    dot_general x16, matrix products, attend(): jnp.einsum('qhd,khd->qhk', query_content, key_content, preferred_element_...  18.9 us
    dot_general x16, matrix products, attend(): jnp.einsum('qhr,kr->qhk', query_rotary, key_rotary, preferred_element_typ...  17.9 us
    unnamed x93, local copies, waits for them, and re-layouts  14.7 us
  transfers between devices with their start and end apart: 15, of which 8 were waited for; matrix products, arithmetic and copies ran while one was open for 6% of the time, Pallas kernels for 0%

commit v1 on v0

v1 whole, which is shorter than its diff:
```python
import functools
import math

import jax
import jax.numpy as jnp
import numpy as np
from jax import lax
from jax.experimental import pallas as pl
from jax.experimental.pallas import tpu as pltpu
from jax.sharding import PartitionSpec as P

NOPE = 128
ROPE = 64
VDIM = 128
GROUP_DIM = 128
SPAN = 16
CHIPS = 4
PEERS = 8

eps_norm = 1e-06
rope_base = 10000.0
masked_score = -1e30

MESH = pl.DeviceIdType.MESH
F32 = jnp.float32
BF16 = jnp.bfloat16
NT = (((1,), (1,)), ((), ()))


def event_list(ring):
    up, down = ring // 2, ring - 1 - ring // 2
    timed = []
    for column in (0, 1):
        first = 0.0 if column == 0 else 4.7
        timed.append((first, (column, 0, 0)))
        base = 0.0 if column == 0 else 5.2
        for k in range(1, up + 1):
            timed.append((base + 2 * k, (column, 0, k)))
        for k in range(1, down + 1):
            timed.append((base + 2 * k + 0.5, (column, 1, k)))
    order = [e for _, e in sorted(timed)]
    at = {e: i for i, e in enumerate(order)}
    next_up, next_down = [], []
    for column, direction, k in order:
        next_up.append(at.get((column, 0, k + 1), 0) if k == 0 or direction == 0 else 0)
        next_down.append(at.get((column, 1, k + 1), 0) if k == 0 or direction == 1 else 0)
    shift = [k if direction == 1 else -k for _, direction, k in order]
    return order, next_up, next_down, shift, at[(1, 0, 0)]


def table(index, entries):
    out = jnp.int32(entries[0])
    for i, entry in enumerate(entries):
        if i > 0 and entry != entries[0]:
            out = jnp.where(index == i, jnp.int32(entry), out)
    return out


def remote(src, dst, send, recv, sp, tp):
    return pltpu.make_async_remote_copy(
        src_ref=src,
        dst_ref=dst,
        send_sem=send,
        recv_sem=recv,
        device_id={"sp": sp, "tp": tp},
        device_id_type=MESH,
    )


def dot(a, b, dims=(((1,), (0,)), ((), ()))):
    return lax.dot_general(a, b, dims, preferred_element_type=F32)


def kernel(
    sp_size,
    tokens,
    mix_gain,
    w_pool_in,
    w_qlat,
    w_kvlat,
    w_krope,
    q_gain,
    kv_gain,
    w_qc,
    w_qr,
    w_key,
    w_value,
    pool_mix,
    pool_scale,
    w_out_pool,
    w_out_attn,
    base_tab,
    rank_tab,
    out,
    logt,
    tok,
    wp,
    wl,
    wqc,
    wqr,
    wk,
    wv,
    mix,
    wo,
    tab,
    proj,
    pool_own,
    halo,
    pool_out,
    kvz,
    kvx,
    qbuf,
    qn,
    qs,
    wk2,
    wv2,
    gk,
    acc,
    stat,
    stat_in,
    stat_wide,
    osum,
    osum_in,
    part,
    rs,
    sem_local,
    sem_ws,
    sem_wr,
    sem_ts,
    sem_tr,
    sem_zs,
    sem_zr,
    sem_xs,
    sem_xr,
    sem_qs,
    sem_qr,
    sem_one_s,
    sem_one_r,
    sem_rs_s,
    sem_rs_r,
):
    sp = lax.axis_index("sp")
    tp = lax.axis_index("tp")
    count = sp_size // SPAN
    ring = SPAN // 2
    x, c = tp // 2, tp % 2
    rank = sp // count
    z, yh = rank // 2, rank % 2
    order, next_up, next_down, shift, y_event = event_list(ring)
    total_events = len(order)
    rows = tokens.shape[0]
    half = rows // 2
    width = tokens.shape[1]
    quarter = half // 4
    own_half = pl.multiple_of(half * c, half)
    other_half = pl.multiple_of(half * (1 - c), half)

    def tp_of(chip, core):
        return lax.rem(chip + CHIPS, CHIPS) * 2 + core

    partner = tp_of(x, 1 - c)
    right, left, across = tp_of(x + 1, c), tp_of(x - 1, c), tp_of(x + 2, c)
    ring_step = 2 * count
    above = lax.rem(sp + ring_step, sp_size)
    below = lax.rem(sp + sp_size - ring_step, sp_size)
    beside = sp + count * (1 - 2 * yh)
    halo_sp = lax.rem(sp + count * c, sp_size)
    halo_greet = lax.rem(sp + sp_size + count * (2 * c - 1), sp_size)

    core64 = pl.multiple_of(64 * c, 64)
    wl_q, wl_kv = core64, pl.multiple_of(128 + 64 * c, 64)
    wo_pool = pl.multiple_of(128 * c, 128)
    wo_attn = pl.multiple_of(256 + 256 * c, 256)
    shared = [
        (w_pool_in, lambda: wp.at[c]),
        (w_qlat, lambda: wl.at[pl.ds(wl_q, 64)]),
        (w_kvlat, lambda: wl.at[pl.ds(wl_kv, 64)]),
        (w_key, lambda: wk.at[c]),
        (w_value, lambda: wv.at[c]),
        (w_qc, lambda: wqc.at[c]),
        (w_qr, lambda: wqr.at[c]),
        (w_out_pool, lambda: wo.at[pl.ds(wo_pool, 128)]),
        (w_out_attn, lambda: wo.at[pl.ds(wo_attn, 256)]),
    ]
    n_shared = len(shared)
    local = [(src, dst()) for src, dst in shared]
    local += [
        (tokens.at[pl.ds(own_half, half)], tok.at[tp]),
        (w_krope, wl.at[pl.ds(256, 64)]),
        (w_krope, wl.at[pl.ds(320, 64)]),
        (base_tab, tab),
        (pool_mix.at[pl.ds(2 * x, 2)], mix),
    ]
    local = [pltpu.make_async_copy(s, d, sem_local.at[i]) for i, (s, d) in enumerate(local)]
    given = [
        remote(s, d(), sem_ws.at[i], sem_wr.at[i], sp, partner) for i, (s, d) in enumerate(shared)
    ]
    for i in [9, 10, 11, 0, 1, 2, 12, 3, 4, 5, 6, 13, 7, 8]:
        local[i].start()

    barrier = pltpu.get_barrier_semaphore()
    for i in range(1, PEERS):
        pl.semaphore_signal(
            barrier, inc=1, device_id={"sp": sp, "tp": lax.rem(tp + i, PEERS)}, device_id_type=MESH
        )
    for other_sp, other_tp in (
        (beside, tp),
        (above, tp),
        (below, tp),
        (halo_greet, partner),
    ):
        pl.semaphore_signal(
            barrier, inc=1, device_id={"sp": other_sp, "tp": other_tp}, device_id_type=MESH
        )
    pl.semaphore_wait(barrier, PEERS - 1 + 4)

    def token_copy(i):
        chip = x + (2, 2, 1, 1, 3, 3, 0)[i]
        core = (0, 1, 0, 1, 0, 1, 1 - c)[i]
        start = pl.multiple_of(half * core, half) if i == 6 else half * core
        return remote(
            tokens.at[pl.ds(start, half)],
            tok.at[tp],
            sem_ts.at[i],
            sem_tr.at[tp],
            sp,
            tp_of(chip, core),
        )

    token_copies = [token_copy(i) for i in range(7)]
    for i in (2, 4, 3, 5, 0, 1, 6):
        token_copies[i].start()
    for g in given:
        g.start()

    local[12].wait()
    lane = lax.broadcasted_iota(jnp.int32, (1, 128), 1)
    low_part = (lane % 64) < 32
    sign = jnp.where(low_part, -1.0, 1.0).astype(F32)
    cos_rank = rank_tab[0, pl.ds(rank, 1), :]
    sin_rank = rank_tab[1, pl.ds(rank, 1), :]
    cos_row, sin_row = tab[0], tab[1]
    tab[0] = cos_row * cos_rank - sin_row * sin_rank
    tab[1] = (sin_row * cos_rank + cos_row * sin_rank) * sign

    def rotate(v, cosine, signed_sine):
        swapped = jnp.where(low_part, pltpu.roll(v, 96, 1), pltpu.roll(v, 32, 1))
        return v * cosine + swapped * signed_sine

    for i in (0, 1, 2, 9, 10, 11):
        local[i].wait()
    for i in (0, 1, 2):
        given[i].wait_recv()

    def slab(j, squares):
        hop = j // 2
        chip = x + jnp.where(hop == 2, 3, jnp.where(hop == 3, 2, hop))
        source = tp_of(chip, (c + j) % 2)

        @pl.when(j > 0)
        def _():
            remote(tok.at[source], tok.at[source], sem_ts.at[0], sem_tr.at[source], sp, partner).wait_recv()

        at = pl.ds(pl.multiple_of(source * width, width), width)
        raw = tok[source].astype(F32)
        scaled = (raw * mix_gain[:, at]).astype(BF16)
        raw = raw * raw
        new = jnp.concatenate(
            [dot(scaled, wp[0, at, :]), dot(scaled, wp[1, at, :]), dot(scaled, wl[:, at], NT)],
            axis=1,
        )

        @pl.when(j == 0)
        def _():
            proj[...] = new

        @pl.when(j > 0)
        def _():
            proj[...] += new

        return squares + raw[:, :128] + raw[:, 128:]

    squares = lax.fori_loop(0, PEERS, slab, jnp.zeros((half, 128), F32))
    inverse = lax.rsqrt(jnp.sum(squares, axis=1, keepdims=True) / (width * PEERS) + eps_norm)
    done = (proj[...] * inverse).astype(BF16)
    own = kvz.at[rank]
    own[:half, :] = done[:, 384:512]
    qbuf[x] = done[:, 256:384]
    pool_own[...] = done[:, :256]
    rope = done[:, 512:640].astype(F32)
    rope = rotate(rope, tab[0, pl.ds(own_half, half), :], tab[1, pl.ds(own_half, half), :])
    rope = jnp.where(lane < 64, rope[: half // 2], rope[half // 2 :])
    own[2 * half :, :] = rope.astype(BF16)

    first = own.at[pl.ds(0, half)]
    to_left = remote(first, own.at[pl.ds(half, half)], sem_zs.at[0], sem_zr.at[0], sp, left)
    to_right = remote(first, kvx.at[rank, 1], sem_xs.at[0, 1], sem_xr.at[0, 1], sp, right)
    to_across = remote(first, kvx.at[rank, 0], sem_xs.at[0, 0], sem_xr.at[0, 0], sp, across)
    q_copies = [
        remote(qbuf.at[x], qbuf.at[x], sem_qs.at[i], sem_qr.at[i], sp, who)
        for i, who in enumerate((left, right, across))
    ]
    q_from = [lax.rem(x + 1, CHIPS), lax.rem(x + 3, CHIPS), lax.rem(x + 2, CHIPS)]
    to_left.start()
    to_right.start()
    to_across.start()
    for q_copy in q_copies:
        q_copy.start()
    halo_copy = remote(
        pool_own.at[pl.ds(half - 16, 16)],
        halo,
        sem_one_s.at[0],
        sem_one_r.at[0],
        halo_sp,
        partner,
    )
    halo_copy.start()

    for i in (3, 4, 5, 6):
        local[i].wait()
        given[i].wait_recv()
    for r in range(CHIPS):
        at = pl.ds(pl.multiple_of(lax.rem(x + r, CHIPS) * 128, 128), 128)
        gk[:, 128 * r : 128 * r + 128] = kv_gain[:, at]
        for core in (0, 1):
            wk2[128 * r : 128 * r + 128, 256 * core : 256 * core + 256] = wk[core, at, :]
            wv2[256 * core : 256 * core + 256, 128 * r : 128 * r + 128] = wv[core, at, :].T

    def block_copy(event, block, to):
        return remote(
            kvz.at[block], kvz.at[block], sem_zs.at[event], sem_zr.at[event], to, tp
        )

    to_left.wait_recv()
    block_copy(next_up[0], rank, above).start()
    if next_down[0]:
        block_copy(next_down[0], rank, below).start()
    block_copy(y_event, rank, beside).start()

    for i, piece in enumerate(q_from):
        remote(
            qbuf.at[piece], qbuf.at[piece], sem_qs.at[i], sem_qr.at[i], sp, left
        ).wait_recv()
    latent = [qbuf[i].astype(F32) for i in range(CHIPS)]
    squares = latent[0] * latent[0]
    for i in range(1, CHIPS):
        squares = squares + latent[i] * latent[i]
    inverse = lax.rsqrt(jnp.sum(squares, axis=1, keepdims=True) / (128 * CHIPS) + eps_norm)
    for i in range(CHIPS):
        gain = q_gain[:, 128 * i : 128 * i + 128]
        qn[pl.ds(own_half, half), 128 * i : 128 * i + 128] = (latent[i] * inverse * gain).astype(BF16)
    qn_copy = remote(
        qn.at[pl.ds(own_half, half)],
        qn.at[pl.ds(own_half, half)],
        sem_one_s.at[1],
        sem_one_r.at[1],
        sp,
        partner,
    )
    qn_copy.start()
    qn_other = qn.at[pl.ds(other_half, half)]
    remote(qn_other, qn_other, sem_one_s.at[1], sem_one_r.at[1], sp, partner).wait_recv()
    normed = qn[...]
    for core in (0, 1):
        content = dot(normed, wqc[core]).astype(BF16)
        rotary = rotate(dot(normed, wqr[core]), tab[0], tab[1])
        for h in (0, 1):
            qs[2 * core + h, :, :128] = content[:, 128 * h : 128 * h + 128]
            mine = (lane < 64) if h == 0 else (lane >= 64)
            qs[2 * core + h, :, 128:] = jnp.where(mine, rotary, 0.0).astype(BF16)

    stat[0:8, :] = jnp.full((8, rows), masked_score, F32)
    stat[8:16, :] = jnp.zeros((8, rows), F32)
    acc[...] = jnp.zeros_like(acc)
    to_log2 = (NOPE + ROPE) ** (-0.5) * math.log2(math.e)

    def rank_of(t):
        column = table(t, [e[0] for e in order])
        moved = table(t, shift)
        return lax.rem(z + moved + ring, ring) * 2 + lax.rem(yh + column, 2)

    def attend(block):
        piece = [
            kvz[block, :half, :].astype(F32),
            kvz[block, half : 2 * half, :].astype(F32),
            kvx[block, 0].astype(F32),
            kvx[block, 1].astype(F32),
        ]
        squares = piece[0] * piece[0]
        for i in range(1, CHIPS):
            squares = squares + piece[i] * piece[i]
        inverse = lax.rsqrt(jnp.sum(squares, axis=1, keepdims=True) / (128 * CHIPS) + eps_norm)
        normed = jnp.concatenate(
            [
                (piece[i] * inverse * gk[:, 128 * i : 128 * i + 128]).astype(BF16)
                for i in range(CHIPS)
            ],
            axis=1,
        )
        content = dot(normed, wk2[...]).astype(BF16)
        values = dot(wv2[...], normed, NT).astype(BF16)
        packed = kvz[block, 2 * half :, :].astype(F32)
        turned = pltpu.roll(packed, 64, 1)
        rotary = jnp.concatenate(
            [jnp.where(lane < 64, packed, turned), jnp.where(lane < 64, turned, packed)], axis=0
        ).astype(BF16)
        ahead = (block - rank) * rows + half * c
        key_at = lax.broadcasted_iota(jnp.int32, (half, rows), 0) + ahead
        allowed = key_at <= lax.broadcasted_iota(jnp.int32, (half, rows), 1)
        for h in range(4):
            keys = jnp.concatenate([content[:, 128 * h : 128 * h + 128], rotary], axis=1)
            scores = dot(keys, qs[h], NT) * to_log2
            scores = jnp.where(allowed, scores, masked_score)
            old = stat[h : h + 1, :]
            new = jnp.maximum(old, jnp.max(scores, axis=0, keepdims=True))
            factor = jnp.exp2(old - new)
            expo = jnp.exp2(scores - new)
            stat[h : h + 1, :] = new
            stat[8 + h : 9 + h, :] = stat[8 + h : 9 + h, :] * factor + jnp.sum(
                expo, axis=0, keepdims=True
            )
            acc[h] = acc[h] * factor + dot(values[128 * h : 128 * h + 128], expo.astype(BF16))

    def pooling():
        remote(halo, halo, sem_one_s.at[0], sem_one_r.at[0], sp, partner).wait_recv()
        local[13].wait()
        before = halo[...].astype(F32)
        before = jnp.where(jnp.logical_and(rank == 0, c == 0), 0.0, before)
        row = lax.broadcasted_iota(jnp.int32, (half, 128), 0) + (rank * rows + own_half)
        odd = x % 2
        for g in (0, 1):
            at = slice(128 * g, 128 * g + 128)
            values = pool_own[:, at].astype(F32)
            extended = jnp.concatenate([before[:, at], values], axis=0)
            sums = [extended]
            for step in (1, 2, 4, 8):
                sums.append(sums[-1] + pltpu.roll(sums[-1], step, 0))
            window = jnp.where(odd == 1, (8, 16)[g], (2, 4)[g])
            chosen = jnp.where(odd == 1, sums[3 + g][16:], sums[1 + g][16:])
            counts = jnp.minimum(row + 1, window).astype(F32)
            pooled = (chosen / counts - values).astype(BF16)
            scale = pool_scale[:, pl.ds(pl.multiple_of(256 * x + 128 * g, 128), 128)]
            pool_out[:, at] = (dot(pooled, mix[g]) * scale).astype(BF16)

    def visit(t, carry):
        @pl.when(t < total_events)
        def _():
            block = rank_of(t)
            block_copy(t, block, above).wait_recv()
            up = table(t, next_up)
            down = table(t, next_down)

            @pl.when(up > 0)
            def _():
                block_copy(up, block, above).start()

            @pl.when(down > 0)
            def _():
                block_copy(down, block, below).start()

            x_copy(t, block, 0).start()
            x_copy(t, block, 1).start()

        earlier = rank_of(t - 1)
        x_copy(t - 1, earlier, 0).wait_recv()
        x_copy(t - 1, earlier, 1).wait_recv()

        @pl.when(earlier <= rank)
        def _():
            attend(earlier)

        @pl.when(t == 2)
        def _():
            pooling()

        return carry

    def x_copy(t, block, which):
        piece = kvz.at[block, pl.ds(half if which == 0 else 0, half)]
        return remote(
            piece,
            kvx.at[block, which],
            sem_xs.at[t, which],
            sem_xr.at[t, which],
            sp,
            left if which == 0 else right,
        )

    lax.fori_loop(1, total_events + 1, visit, 0)

    for h in range(4):
        osum[:, 128 * h : 128 * h + 128] = acc[h].T
    stat_wide[0:16, :] = stat[...]
    stat_wide[16:128, :] = jnp.zeros((112, rows), F32)
    osum[:, 512:640] = stat_wide[...].T
    osum_copy = remote(
        osum.at[pl.ds(other_half, half)], osum_in, sem_one_s.at[2], sem_one_r.at[2], sp, partner
    )
    stat_copy = remote(stat, stat_in, sem_one_s.at[3], sem_one_r.at[3], sp, partner)
    osum_copy.start()
    stat_copy.start()
    for i in (7, 8):
        local[i].wait()
        given[i].wait_recv()
    stat_copy.wait_recv()
    most = jnp.maximum(stat[0:8, :], stat_in[0:8, :])
    sums = stat[8:16, :] * jnp.exp2(stat[0:8, :] - most) + stat_in[8:16, :] * jnp.exp2(
        stat_in[0:8, :] - most
    )
    logs = most * math.log(2.0) + jnp.log(sums)
    logt[...] = jnp.where(c == 0, logs[0:2, :], logs[2:4, :])
    osum_copy.wait_recv()
    own_rows = pl.ds(own_half, half)
    mixed = [pool_out[...]]
    own_stat, other_stat = osum[own_rows, 512:640], osum_in[:, 512:640]
    for h in range(4):
        at = slice(128 * h, 128 * h + 128)
        own_max, other_max = own_stat[:, h : h + 1], other_stat[:, h : h + 1]
        most = jnp.maximum(own_max, other_max)
        own_factor, other_factor = jnp.exp2(own_max - most), jnp.exp2(other_max - most)
        sums = (
            own_stat[:, 8 + h : 9 + h] * own_factor + other_stat[:, 8 + h : 9 + h] * other_factor
        )
        mixed.append(
            (
                (osum[own_rows, at] * own_factor + osum_in[:, at] * other_factor) / sums
            ).astype(BF16)
        )
    mixed = jnp.concatenate(mixed, axis=1)

    columns = wo.shape[1]
    chunks = sem_rs_s.shape[1]
    chunk = columns // chunks
    mine = x // 2 == c

    def part_copy(i, n):
        at = pl.ds(n * chunk, chunk)
        return remote(
            part.at[pl.ds(quarter * i, quarter), at],
            rs.at[x, :, at],
            sem_rs_s.at[i, n],
            sem_rs_r.at[x, n],
            sp,
            4 * c + i,
        )

    own_at = pl.multiple_of(quarter * lax.rem(tp, 4), quarter)

    def part_keep(n):
        at = pl.ds(n * chunk, chunk)
        return pltpu.make_async_copy(
            part.at[pl.ds(own_at, quarter), at], rs.at[x, :, at], sem_local.at[14 + n]
        )

    for n in range(chunks):
        at = slice(n * chunk, (n + 1) * chunk)
        part[:, at] = dot(mixed, wo[:, at]).astype(BF16)
        for i in range(4):

            @pl.when(4 * c + i != tp)
            def _():
                part_copy(i, n).start()

        @pl.when(mine)
        def _():
            part_keep(n).start()

    for n in range(chunks):
        at = slice(n * chunk, (n + 1) * chunk)
        for chip in range(CHIPS):

            @pl.when(jnp.logical_and(mine, x == chip))
            def _():
                part_keep(n).wait()

            @pl.when(jnp.logical_not(jnp.logical_and(mine, x == chip)))
            def _():
                ref = rs.at[chip, :, pl.ds(n * chunk, chunk)]
                remote(ref, ref, sem_rs_s.at[0, n], sem_rs_r.at[chip, n], sp, partner).wait_recv()

        out[:, at] = (
            rs[0, :, at].astype(F32)
            + rs[1, :, at].astype(F32)
            + rs[2, :, at].astype(F32)
            + rs[3, :, at].astype(F32)
        ).astype(BF16)

    for cp in token_copies + given + q_copies:
        cp.wait_send()
    to_left.wait_send()
    to_right.wait_send()
    to_across.wait_send()
    for cp in (halo_copy, qn_copy, osum_copy, stat_copy):
        cp.wait_send()

    def drain(t, carry):
        block_copy(t, 0, above).wait_send()
        x_copy(t, 0, 0).wait_send()
        x_copy(t, 0, 1).wait_send()
        return carry

    lax.fori_loop(1, total_events, drain, 0)
    for n in range(chunks):
        for i in range(4):

            @pl.when(4 * c + i != tp)
            def _():
                part_copy(i, n).wait_send()


def rotary_tables(rows, ranks):
    frequency = rope_base ** (-np.arange(ROPE // 2, dtype=np.float64) * 2.0 / ROPE)
    frequency = np.tile(frequency, 128 // (ROPE // 2))
    by_row = np.arange(rows)[:, None] * frequency[None, :]
    by_rank = (np.arange(ranks) * rows)[:, None] * frequency[None, :]
    return (
        np.stack([np.cos(by_row), np.sin(by_row)]).astype(np.float32),
        np.stack([np.cos(by_rank), np.sin(by_rank)]).astype(np.float32),
    )


def per_device(
    sp_size,
    tokens,
    mix_gain,
    w_pool_in,
    w_qlat,
    w_kvlat,
    w_krope,
    q_gain,
    kv_gain,
    w_q_content,
    w_q_rotary,
    w_key,
    w_value,
    pool_mix,
    pool_scale,
    w_out_pool,
    w_out_attn,
):
    rows, width = tokens.shape
    half = rows // 2
    columns = w_out_attn.shape[1]
    features = width * PEERS
    base_tab, rank_tab = rotary_tables(rows, SPAN)
    total_events = len(event_list(SPAN // 2)[0])
    chunks = 2
    anywhere = pl.BlockSpec(memory_space=pl.ANY)
    near = pl.BlockSpec(memory_space=pltpu.VMEM)
    dma = lambda *shape: pltpu.SemaphoreType.DMA(shape)
    vmem = pltpu.VMEM
    out, logt = pl.pallas_call(
        functools.partial(kernel, sp_size),
        out_shape=(
            jax.ShapeDtypeStruct((rows // PEERS, columns), BF16),
            jax.ShapeDtypeStruct((2, rows), F32),
        ),
        in_specs=[
            anywhere,
            near,
            anywhere,
            anywhere,
            anywhere,
            anywhere,
            near,
            near,
            anywhere,
            anywhere,
            anywhere,
            anywhere,
            anywhere,
            near,
            anywhere,
            anywhere,
            anywhere,
            near,
        ],
        out_specs=(near, near),
        scratch_shapes=[
            vmem((PEERS, half, width), BF16),
            vmem((2, features, 128), BF16),
            vmem((384, features), BF16),
            vmem((2, 512, 256), BF16),
            vmem((2, 512, 128), BF16),
            vmem((2, 512, 256), BF16),
            vmem((2, 512, 256), BF16),
            vmem((2, 128, 128), BF16),
            vmem((768, columns), BF16),
            vmem((2, rows, 128), F32),
            vmem((half, 640), F32),
            vmem((half, 256), BF16),
            vmem((16, 256), BF16),
            vmem((half, 256), BF16),
            vmem((SPAN, 2 * half + half // 2, 128), BF16),
            vmem((SPAN, 2, half, 128), BF16),
            vmem((CHIPS, half, 128), BF16),
            vmem((rows, 512), BF16),
            vmem((4, rows, 256), BF16),
            vmem((512, 512), BF16),
            vmem((512, 512), BF16),
            vmem((1, 512), F32),
            vmem((4, 128, rows), F32),
            vmem((16, rows), F32),
            vmem((16, rows), F32),
            vmem((128, rows), F32),
            vmem((rows, 640), F32),
            vmem((half, 640), F32),
            vmem((half, columns), BF16),
            vmem((CHIPS, rows // PEERS, columns), BF16),
            dma(14 + chunks),
            dma(9),
            dma(9),
            dma(7),
            dma(PEERS),
            dma(total_events),
            dma(total_events),
            dma(total_events, 2),
            dma(total_events, 2),
            dma(3),
            dma(3),
            dma(4),
            dma(4),
            dma(4, chunks),
            dma(CHIPS, chunks),
        ],
        compiler_params=pltpu.CompilerParams(
            collective_id=0, has_side_effects=True, vmem_limit_bytes=56 * 1024 * 1024
        ),
    )(
        tokens,
        mix_gain.reshape(1, -1),
        w_pool_in,
        w_qlat.T,
        w_kvlat.T,
        w_krope.T,
        q_gain.reshape(1, -1),
        kv_gain.reshape(1, -1),
        w_q_content,
        w_q_rotary,
        w_key,
        w_value,
        pool_mix,
        pool_scale.reshape(1, -1),
        w_out_pool,
        w_out_attn,
        jnp.asarray(base_tab),
        jnp.asarray(rank_tab),
    )
    return out, logt.T


def solution(mesh):
    in_specs = (
        P("sp", "tp"),
        P(),
        P(None, "tp"),
        P(None, "tp"),
        P(None, "tp"),
        P(),
        P(),
        P(),
        P(None, "tp"),
        P(None, "tp"),
        P(None, "tp"),
        P(None, "tp"),
        P(),
        P(),
        P("tp", None),
        P("tp", None),
    )
    out_specs = (P(("sp", "tp"), None), P("sp", "tp"))
    return jax.shard_map(
        functools.partial(per_device, mesh.shape["sp"]),
        mesh=mesh,
        in_specs=in_specs,
        out_specs=out_specs,
        check_vma=False,
    )
```

time: 447 us -> 95 us (0.21)
  the two profiles are of different devices: /device:TPU:128 before, /device:TPU:1 now
where the time goes in v1:
time: 95 us; the launch traced here: 94.8 us
  Pallas kernels  92 us (97%)
  local copies, waits for them, and re-layouts  2.2 us (2%)
    pallas_call x1, Pallas kernels, per_device(): pl.pallas_call(functools.partial(kernel, sp_size), out_shape=(jax.ShapeDt...  92 us
    unnamed x4, local copies, waits for them, and re-layouts  2.2 us

profile of v1, /device:TPU:1, one launch (start us, length us, event | category | flops | bytes accessed | tf_op | source)
XLA Modules:
  0.0 94.8 jit_solution(12690768317058582741)
XLA Ops:
  0.6 92.0 %shard_map.185 = (bf16[48,2048]{1,0:T(8,128)(2,1)}, f32[2,384]{1,0:T(2,128)}) custom-call(bf16[384,256]{1,0:T(8,128)(2,1)} %tokens.1, f32[1,2048]{1,0:T(1,128)} %bitcast.11, bf16[2048,128]{1,0:T(8,128)(2,1)} %w_pool_in.1, bf16[64,2048]{1,0:T(8,128)(2,1)} %bitcast.8, bf16[64,2048]{1,0:T(8,128)(2,1)} %bitcast.9, bf16[64,2048]{1,0:T(8,128)(2,1)} %bitcast.10, ...), custom_call_target="tpu_custom_call" | custom-call | tf_op jit(solution)/shard_map/pallas_call | solution.py:652
  92.6 0.0 copy-start
  92.6 1.6 %copy.22 = bf16[48,2048]{1,0:T(8,128)(2,1)} copy(bf16[48,2048]{1,0:T(8,128)(2,1)} %get-tuple-element.8) | data formatting | bytes 393216
  94.2 0.0 copy-done
  94.2 0.6 copy.23
Async XLA Ops:
  92.6 1.6 %copy-start = (f32[2,384]{1,0:T(2,128)S(1)}, f32[2,384]{1,0:T(2,128)}, u32[]{:S(2)}) copy-start(f32[2,384]{1,0:T(2,128)} %get-tuple-element.5) | copy-start | bytes 9220

commit v2 on v1

--- a/solution.py
+++ b/solution.py
@@ -28,24 +28,32 @@
 
 
 def event_list(ring):
-    up, down = ring // 2, ring - 1 - ring // 2
+    far = ring // 2
     timed = []
     for column in (0, 1):
-        first = 0.0 if column == 0 else 4.7
+        first, pace = (0.0, 4.5) if column == 0 else (10.0, 4.7)
         timed.append((first, (column, 0, 0)))
-        base = 0.0 if column == 0 else 5.2
-        for k in range(1, up + 1):
-            timed.append((base + 2 * k, (column, 0, k)))
-        for k in range(1, down + 1):
-            timed.append((base + 2 * k + 0.5, (column, 1, k)))
+        for k in range(1, far):
+            timed.append((first + pace * k, (column, 0, k)))
+            timed.append((first + pace * k + 0.1, (column, 1, k)))
+        timed.append((first + pace * far, (column, 2, far)))
     order = [e for _, e in sorted(timed)]
     at = {e: i for i, e in enumerate(order)}
-    next_up, next_down = [], []
-    for column, direction, k in order:
-        next_up.append(at.get((column, 0, k + 1), 0) if k == 0 or direction == 0 else 0)
-        next_down.append(at.get((column, 1, k + 1), 0) if k == 0 or direction == 1 else 0)
+    follow = {}
+    for going in (0, 1):
+        for which in (0, 1):
+            entries = []
+            for column, direction, k in order:
+                entry = 0
+                if k == 0 or direction == going:
+                    if k + 1 < far:
+                        entry = at[(column, going, k + 1)]
+                    elif which == going:
+                        entry = at[(column, 2, far)]
+                entries.append(entry)
+            follow[going, which] = entries
     shift = [k if direction == 1 else -k for _, direction, k in order]
-    return order, next_up, next_down, shift, at[(1, 0, 0)]
+    return order, follow, shift, at[(1, 0, 0)]
 
 
 def table(index, entries):
@@ -115,12 +123,15 @@
     wk2,
     wv2,
     gk,
+    content_at,
+    values_at,
+    rotary_at,
     acc,
     stat,
     stat_in,
-    stat_wide,
-    osum,
-    osum_in,
+    most_at,
+    sum_at,
+    acc_in,
     part,
     rs,
     sem_local,
@@ -146,7 +157,7 @@
     x, c = tp // 2, tp % 2
     rank = sp // count
     z, yh = rank // 2, rank % 2
-    order, next_up, next_down, shift, y_event = event_list(ring)
+    order, follow, shift, y_event = event_list(ring)
     total_events = len(order)
     rows = tokens.shape[0]
     half = rows // 2
@@ -290,10 +301,23 @@
     rope = done[:, 512:640].astype(F32)
     rope = rotate(rope, tab[0, pl.ds(own_half, half), :], tab[1, pl.ds(own_half, half), :])
     rope = jnp.where(lane < 64, rope[: half // 2], rope[half // 2 :])
-    own[2 * half :, :] = rope.astype(BF16)
+    own[half : half + half // 2, :] = rope.astype(BF16)
+
+    first_part = pl.ds(0, half + half // 2)
+    second = pl.ds(half + half // 2, half)
+
+    def block_copy(event, which, block, to):
+        piece = kvz.at[block, first_part if which == 0 else second]
+        return remote(piece, piece, sem_zs.at[event, which], sem_zr.at[event, which], to, tp)
+
+    def start_own(which):
+        for going, to in ((0, above), (1, below)):
+            if follow[going, which][0]:
+                block_copy(follow[going, which][0], which, rank, to).start()
+        block_copy(y_event, which, rank, beside).start()
 
     first = own.at[pl.ds(0, half)]
-    to_left = remote(first, own.at[pl.ds(half, half)], sem_zs.at[0], sem_zr.at[0], sp, left)
+    to_left = remote(first, own.at[second], sem_zs.at[0, 1], sem_zr.at[0, 1], sp, left)
     to_right = remote(first, kvx.at[rank, 1], sem_xs.at[0, 1], sem_xr.at[0, 1], sp, right)
     to_across = remote(first, kvx.at[rank, 0], sem_xs.at[0, 0], sem_xr.at[0, 0], sp, across)
     q_copies = [
@@ -302,6 +326,7 @@
     ]
     q_from = [lax.rem(x + 1, CHIPS), lax.rem(x + 3, CHIPS), lax.rem(x + 2, CHIPS)]
     to_left.start()
+    start_own(0)
     to_right.start()
     to_across.start()
     for q_copy in q_copies:
@@ -324,19 +349,46 @@
         gk[:, 128 * r : 128 * r + 128] = kv_gain[:, at]
         for core in (0, 1):
             wk2[128 * r : 128 * r + 128, 256 * core : 256 * core + 256] = wk[core, at, :]
-            wv2[256 * core : 256 * core + 256, 128 * r : 128 * r + 128] = wv[core, at, :].T
-
-    def block_copy(event, block, to):
+            wv2[128 * r : 128 * r + 128, 256 * core : 256 * core + 256] = wv[core, at, :]
+
+    def rank_of(t):
+        column = table(t, [e[0] for e in order])
+        moved = table(t, shift)
+        return lax.rem(z + moved + ring, ring) * 2 + lax.rem(yh + column, 2)
+
+    def x_copy(t, block, which):
+        piece = kvz.at[block, second if which == 0 else pl.ds(0, half)]
         return remote(
-            kvz.at[block], kvz.at[block], sem_zs.at[event], sem_zr.at[event], to, tp
+            piece,
+            kvx.at[block, which],
+            sem_xs.at[t, which],
+            sem_xr.at[t, which],
+            sp,
+            left if which == 0 else right,
         )
 
+    def forward(t):
+        block = rank_of(t)
+        for which in (0, 1):
+            block_copy(t, which, block, above).wait_recv()
+            for going, to in ((0, above), (1, below)):
+                entry = table(t, follow[going, which])
+
+                @pl.when(entry > 0)
+                def _():
+                    block_copy(entry, which, block, to).start()
+
+            x_copy(t, block, 1 - which).start()
+
+    def arrived(t, block):
+        x_copy(t, block, 0).wait_recv()
+        x_copy(t, block, 1).wait_recv()
+
     to_left.wait_recv()
-    block_copy(next_up[0], rank, above).start()
-    if next_down[0]:
-        block_copy(next_down[0], rank, below).start()
-    block_copy(y_event, rank, beside).start()
-
+    start_own(1)
+
+    forward(jnp.int32(1))
+    forward(jnp.int32(2))
     for i, piece in enumerate(q_from):
         remote(
             qbuf.at[piece], qbuf.at[piece], sem_qs.at[i], sem_qr.at[i], sp, left
@@ -361,30 +413,27 @@
     qn_other = qn.at[pl.ds(other_half, half)]
     remote(qn_other, qn_other, sem_one_s.at[1], sem_one_r.at[1], sp, partner).wait_recv()
     normed = qn[...]
+    to_log2 = (NOPE + ROPE) ** (-0.5) * math.log2(math.e)
     for core in (0, 1):
-        content = dot(normed, wqc[core]).astype(BF16)
-        rotary = rotate(dot(normed, wqr[core]), tab[0], tab[1])
+        content = (dot(normed, wqc[core]) * to_log2).astype(BF16)
+        rotary = rotate(dot(normed, wqr[core]), tab[0], tab[1]) * to_log2
         for h in (0, 1):
             qs[2 * core + h, :, :128] = content[:, 128 * h : 128 * h + 128]
-            mine = (lane < 64) if h == 0 else (lane >= 64)
-            qs[2 * core + h, :, 128:] = jnp.where(mine, rotary, 0.0).astype(BF16)
-
-    stat[0:8, :] = jnp.full((8, rows), masked_score, F32)
-    stat[8:16, :] = jnp.zeros((8, rows), F32)
+            turned = rotary if h == 0 else pltpu.roll(rotary, 64, 1)
+            spare = jnp.where(lane == 64, 1.0, 0.0)
+            qs[2 * core + h, :, 128:] = jnp.where(lane < 64, turned, spare).astype(BF16)
+
+    most_at[...] = jnp.full(most_at.shape, masked_score, F32)
+    sum_at[...] = jnp.zeros_like(sum_at)
     acc[...] = jnp.zeros_like(acc)
-    to_log2 = (NOPE + ROPE) ** (-0.5) * math.log2(math.e)
-
-    def rank_of(t):
-        column = table(t, [e[0] for e in order])
-        moved = table(t, shift)
-        return lax.rem(z + moved + ring, ring) * 2 + lax.rem(yh + column, 2)
-
-    def attend(block):
+
+    def expand(blocks):
+        parts = (pl.ds(0, half), second)
         piece = [
-            kvz[block, :half, :].astype(F32),
-            kvz[block, half : 2 * half, :].astype(F32),
-            kvx[block, 0].astype(F32),
-            kvx[block, 1].astype(F32),
+            jnp.concatenate([kvz[b, at, :].astype(F32) for b in blocks], axis=0) for at in parts
+        ]
+        piece += [
+            jnp.concatenate([kvx[b, i].astype(F32) for b in blocks], axis=0) for i in (0, 1)
         ]
         squares = piece[0] * piece[0]
         for i in range(1, CHIPS):
@@ -398,28 +447,38 @@
             axis=1,
         )
         content = dot(normed, wk2[...]).astype(BF16)
-        values = dot(wv2[...], normed, NT).astype(BF16)
-        packed = kvz[block, 2 * half :, :].astype(F32)
-        turned = pltpu.roll(packed, 64, 1)
-        rotary = jnp.concatenate(
-            [jnp.where(lane < 64, packed, turned), jnp.where(lane < 64, turned, packed)], axis=0
-        ).astype(BF16)
-        ahead = (block - rank) * rows + half * c
-        key_at = lax.broadcasted_iota(jnp.int32, (half, rows), 0) + ahead
-        allowed = key_at <= lax.broadcasted_iota(jnp.int32, (half, rows), 1)
-        for h in range(4):
-            keys = jnp.concatenate([content[:, 128 * h : 128 * h + 128], rotary], axis=1)
-            scores = dot(keys, qs[h], NT) * to_log2
-            scores = jnp.where(allowed, scores, masked_score)
-            old = stat[h : h + 1, :]
-            new = jnp.maximum(old, jnp.max(scores, axis=0, keepdims=True))
+        values = dot(normed, wv2[...]).astype(BF16)
+        rotary = []
+        for b in blocks:
+            packed = kvz[b, half : half + half // 2, :].astype(F32)
+            hidden = jnp.where(b <= rank, 0.0, masked_score).astype(F32)
+            spare = jnp.where(lane == 64, hidden, 0.0)
+            rotary.append(jnp.where(lane < 64, packed, spare))
+            rotary.append(jnp.where(lane < 64, pltpu.roll(packed, 64, 1), spare))
+        rotary = jnp.concatenate(rotary, axis=0).astype(BF16)
+        content_at[...] = content
+        values_at[...] = values
+        rotary_at[...] = rotary
+
+    def attend_heads(heads, masked):
+        if masked:
+            column = lax.broadcasted_iota(jnp.int32, (rows, rows), 1)
+            row = lax.broadcasted_iota(jnp.int32, (rows, rows), 0)
+            allowed = jnp.logical_or(column >= half, column + half * c <= row)
+        for h in heads:
+            at = slice(128 * h, 128 * h + 128)
+            keys = jnp.concatenate([content_at[:, at], rotary_at[...]], axis=1)
+            scores = dot(qs[h], keys, NT)
+            if masked:
+                scores = jnp.where(allowed, scores, masked_score)
+            old = most_at[h]
+            new = jnp.maximum(old, jnp.max(scores, axis=1, keepdims=True))
             factor = jnp.exp2(old - new)
-            expo = jnp.exp2(scores - new)
-            stat[h : h + 1, :] = new
-            stat[8 + h : 9 + h, :] = stat[8 + h : 9 + h, :] * factor + jnp.sum(
-                expo, axis=0, keepdims=True
-            )
-            acc[h] = acc[h] * factor + dot(values[128 * h : 128 * h + 128], expo.astype(BF16))
+            expo = [jnp.exp2(scores[:, i : i + 128] - new) for i in range(0, rows, 128)]
+            most_at[h] = new
+            sum_at[h] = sum_at[h] * factor + sum(expo[1:], expo[0])
+            expo = jnp.concatenate([e.astype(BF16) for e in expo], axis=1)
+            acc[h] = acc[h] * factor + dot(expo, values_at[:, at])
 
     def pooling():
         remote(halo, halo, sem_one_s.at[0], sem_one_r.at[0], sp, partner).wait_recv()
@@ -442,90 +501,80 @@
             scale = pool_scale[:, pl.ds(pl.multiple_of(256 * x + 128 * g, 128), 128)]
             pool_out[:, at] = (dot(pooled, mix[g]) * scale).astype(BF16)
 
-    def visit(t, carry):
-        @pl.when(t < total_events)
+    forward(jnp.int32(3))
+    arrived(0, rank)
+    arrived(1, rank_of(jnp.int32(1)))
+    expand([rank, rank_of(jnp.int32(1))])
+    attend_heads((0, 1), True)
+    forward(jnp.int32(4))
+    attend_heads((2, 3), True)
+
+    def visit(i, carry):
+        @pl.when(2 * i + 3 < total_events)
         def _():
-            block = rank_of(t)
-            block_copy(t, block, above).wait_recv()
-            up = table(t, next_up)
-            down = table(t, next_down)
-
-            @pl.when(up > 0)
-            def _():
-                block_copy(up, block, above).start()
-
-            @pl.when(down > 0)
-            def _():
-                block_copy(down, block, below).start()
-
-            x_copy(t, block, 0).start()
-            x_copy(t, block, 1).start()
-
-        earlier = rank_of(t - 1)
-        x_copy(t - 1, earlier, 0).wait_recv()
-        x_copy(t - 1, earlier, 1).wait_recv()
-
-        @pl.when(earlier <= rank)
+            forward(2 * i + 3)
+
+        earlier = [rank_of(2 * i), rank_of(2 * i + 1)]
+        seen = jnp.logical_or(earlier[0] < rank, earlier[1] < rank)
+        arrived(2 * i, earlier[0])
+        arrived(2 * i + 1, earlier[1])
+
+        @pl.when(seen)
         def _():
-            attend(earlier)
-
-        @pl.when(t == 2)
+            expand(earlier)
+            attend_heads((0, 1), False)
+
+
+        @pl.when(2 * i + 4 < total_events)
+        def _():
+            forward(2 * i + 4)
+
+
+        @pl.when(seen)
+        def _():
+            attend_heads((2, 3), False)
+
+        @pl.when(i == 1)
         def _():
             pooling()
 
         return carry
 
-    def x_copy(t, block, which):
-        piece = kvz.at[block, pl.ds(half if which == 0 else 0, half)]
-        return remote(
-            piece,
-            kvx.at[block, which],
-            sem_xs.at[t, which],
-            sem_xr.at[t, which],
-            sp,
-            left if which == 0 else right,
-        )
-
-    lax.fori_loop(1, total_events + 1, visit, 0)
-
+    lax.fori_loop(1, total_events // 2, visit, 0)
+
+    acc_copy = remote(
+        acc.at[:, pl.ds(other_half, half), :], acc_in, sem_one_s.at[2], sem_one_r.at[2], sp, partner
+    )
+    acc_copy.start()
+    packed = jnp.zeros((rows, 128), F32)
     for h in range(4):
-        osum[:, 128 * h : 128 * h + 128] = acc[h].T
-    stat_wide[0:16, :] = stat[...]
-    stat_wide[16:128, :] = jnp.zeros((112, rows), F32)
-    osum[:, 512:640] = stat_wide[...].T
-    osum_copy = remote(
-        osum.at[pl.ds(other_half, half)], osum_in, sem_one_s.at[2], sem_one_r.at[2], sp, partner
-    )
+        packed = jnp.where(lane == h, most_at[h], packed)
+        packed = jnp.where(lane == 8 + h, jnp.sum(sum_at[h], axis=1, keepdims=True), packed)
+    stat[...] = packed
     stat_copy = remote(stat, stat_in, sem_one_s.at[3], sem_one_r.at[3], sp, partner)
-    osum_copy.start()
     stat_copy.start()
     for i in (7, 8):
         local[i].wait()
         given[i].wait_recv()
     stat_copy.wait_recv()
-    most = jnp.maximum(stat[0:8, :], stat_in[0:8, :])
-    sums = stat[8:16, :] * jnp.exp2(stat[0:8, :] - most) + stat_in[8:16, :] * jnp.exp2(
-        stat_in[0:8, :] - most
-    )
-    logs = most * math.log(2.0) + jnp.log(sums)
+    acc_copy.wait_recv()
+    own_rows = pl.ds(own_half, half)
+    mine_now, other_now = stat[...], stat_in[...]
+    most = jnp.maximum(mine_now, other_now)
+    sum_at[0] = jnp.exp2(mine_now - most)
+    sum_at[1] = jnp.exp2(other_now - most)
+    sums = pltpu.roll(mine_now, 120, 1) * sum_at[0] + pltpu.roll(other_now, 120, 1) * sum_at[1]
+    sums = jnp.where(lane < 4, sums, 1.0)
+    logs = jnp.where(lane < 4, most, 0.0) * math.log(2.0) + jnp.log(sums)
+    logs = logs.T
     logt[...] = jnp.where(c == 0, logs[0:2, :], logs[2:4, :])
-    osum_copy.wait_recv()
-    own_rows = pl.ds(own_half, half)
+    most_at[0] = 1.0 / sums
     mixed = [pool_out[...]]
-    own_stat, other_stat = osum[own_rows, 512:640], osum_in[:, 512:640]
     for h in range(4):
-        at = slice(128 * h, 128 * h + 128)
-        own_max, other_max = own_stat[:, h : h + 1], other_stat[:, h : h + 1]
-        most = jnp.maximum(own_max, other_max)
-        own_factor, other_factor = jnp.exp2(own_max - most), jnp.exp2(other_max - most)
-        sums = (
-            own_stat[:, 8 + h : 9 + h] * own_factor + other_stat[:, 8 + h : 9 + h] * other_factor
-        )
-        mixed.append(
-            (
-                (osum[own_rows, at] * own_factor + osum_in[:, at] * other_factor) / sums
-            ).astype(BF16)
-        )
+        share = most_at[0, own_rows, h : h + 1]
+        own_share = sum_at[0, own_rows, h : h + 1] * share
+        other_share = sum_at[1, own_rows, h : h + 1] * share
+        mixed.append((acc[h, own_rows, :] * own_share + acc_in[h] * other_share).astype(BF16))
     mixed = jnp.concatenate(mixed, axis=1)
 
     columns = wo.shape[1]
@@ -590,11 +639,12 @@
     to_left.wait_send()
     to_right.wait_send()
     to_across.wait_send()
-    for cp in (halo_copy, qn_copy, osum_copy, stat_copy):
+    for cp in (halo_copy, qn_copy, acc_copy, stat_copy):
         cp.wait_send()
 
     def drain(t, carry):
-        block_copy(t, 0, above).wait_send()
+        block_copy(t, 0, 0, above).wait_send()
+        block_copy(t, 1, 0, above).wait_send()
         x_copy(t, 0, 0).wait_send()
         x_copy(t, 0, 1).wait_send()
         return carry
@@ -699,12 +749,15 @@
             vmem((512, 512), BF16),
             vmem((512, 512), BF16),
             vmem((1, 512), F32),
-            vmem((4, 128, rows), F32),
-            vmem((16, rows), F32),
-            vmem((16, rows), F32),
-            vmem((128, rows), F32),
-            vmem((rows, 640), F32),
-            vmem((half, 640), F32),
+            vmem((rows, 512), BF16),
+            vmem((rows, 512), BF16),
+            vmem((rows, 128), BF16),
+            vmem((4, rows, 128), F32),
+            vmem((rows, 128), F32),
+            vmem((rows, 128), F32),
+            vmem((4, rows, 128), F32),
+            vmem((4, rows, 128), F32),
+            vmem((4, half, 128), F32),
             vmem((half, columns), BF16),
             vmem((CHIPS, rows // PEERS, columns), BF16),
             dma(14 + chunks),
@@ -712,8 +765,8 @@
             dma(9),
             dma(7),
             dma(PEERS),
-            dma(total_events),
-            dma(total_events),
+            dma(total_events, 2),
+            dma(total_events, 2),
             dma(total_events, 2),
             dma(total_events, 2),
             dma(3),

time: 95 us -> 80.6 us (0.85)
  Pallas kernels: 92 us -> 77.6 us
    pallas_call x1, Pallas kernels: 92 us -> 77.6 us  [per_device(): pl.pallas_call(functools.partial(kernel, sp_size), out_shape=(jax.ShapeDt...]
where the time goes in v2:
time: 80.6 us; the launch traced here: 80.4 us
  Pallas kernels  77.6 us (96%)
  local copies, waits for them, and re-layouts  2.2 us (3%)
    pallas_call x1, Pallas kernels, per_device(): pl.pallas_call(functools.partial(kernel, sp_size), out_shape=(jax.ShapeDt...  77.6 us
    unnamed x4, local copies, waits for them, and re-layouts  2.2 us

profile of v2, /device:TPU:1, one launch (start us, length us, event | category | flops | bytes accessed | tf_op | source)
XLA Modules:
  0.0 80.4 jit_solution(8214100350298211881)
XLA Ops:
  0.6 77.6 %shard_map.185 = (bf16[48,2048]{1,0:T(8,128)(2,1)}, f32[2,384]{1,0:T(2,128)}) custom-call(bf16[384,256]{1,0:T(8,128)(2,1)} %tokens.1, f32[1,2048]{1,0:T(1,128)} %bitcast.11, bf16[2048,128]{1,0:T(8,128)(2,1)} %w_pool_in.1, bf16[64,2048]{1,0:T(8,128)(2,1)} %bitcast.8, bf16[64,2048]{1,0:T(8,128)(2,1)} %bitcast.9, bf16[64,2048]{1,0:T(8,128)(2,1)} %bitcast.10, ...), custom_call_target="tpu_custom_call" | custom-call | tf_op jit(solution)/shard_map/pallas_call | solution.py:702
  78.2 0.0 copy-start
  78.2 1.6 %copy.22 = bf16[48,2048]{1,0:T(8,128)(2,1)} copy(bf16[48,2048]{1,0:T(8,128)(2,1)} %get-tuple-element.8) | data formatting | bytes 393216
  79.9 0.0 copy-done
  79.9 0.6 copy.23
Async XLA Ops:
  78.2 1.6 %copy-start = (f32[2,384]{1,0:T(2,128)S(1)}, f32[2,384]{1,0:T(2,128)}, u32[]{:S(2)}) copy-start(f32[2,384]{1,0:T(2,128)} %get-tuple-element.5) | copy-start | bytes 9220

commit v3 on v2

--- a/solution.py
+++ b/solution.py
@@ -53,10 +53,30 @@
                 entries.append(entry)
             follow[going, which] = entries
     shift = [k if direction == 1 else -k for _, direction, k in order]
-    return order, follow, shift, at[(1, 0, 0)]
+    limit = ([], [])
+    parent = ([], [])
+    for which in (0, 1):
+        for column, direction, k in order:
+            bound = (ring - k, far - 1 + which, far)[direction]
+            limit[which].append(bound)
+            before = at[(column, direction if direction < 2 else which, k - 1)] if k > 1 else 0
+            parent[which].append(at[(column, 0, 0)] if k == 1 else before)
+    next_limit = {
+        key: [limit[key[1]][e] if e else 0 for e in entries] for key, entries in follow.items()
+    }
+    when = {e: t for t, e in timed}
+    pairs = []
+    for above in (False, True):
+        group = [e for e in order if (e[1] == 1) == above]
+        pairs += list(zip(group[::2], group[1::2]))
+    pairs.sort(key=lambda pair: when[pair[1]])
+    pairs = [[at[e] for e in pair] for pair in pairs]
+    return order, follow, shift, at[(1, 0, 0)], limit, next_limit, parent, pairs
 
 
 def table(index, entries):
+    if isinstance(index, int):
+        return entries[index]
     out = jnp.int32(entries[0])
     for i, entry in enumerate(entries):
         if i > 0 and entry != entries[0]:
@@ -157,7 +177,7 @@
     x, c = tp // 2, tp % 2
     rank = sp // count
     z, yh = rank // 2, rank % 2
-    order, follow, shift, y_event = event_list(ring)
+    order, follow, shift, y_event, limit, next_limit, parent, pairs = event_list(ring)
     total_events = len(order)
     rows = tokens.shape[0]
     half = rows // 2
@@ -313,7 +333,11 @@
     def start_own(which):
         for going, to in ((0, above), (1, below)):
             if follow[going, which][0]:
-                block_copy(follow[going, which][0], which, rank, to).start()
+
+                @pl.when(z < next_limit[going, which][0])
+                def _():
+                    block_copy(follow[going, which][0], which, rank, to).start()
+
         block_copy(y_event, which, rank, beside).start()
 
     first = own.at[pl.ds(0, half)]
@@ -367,22 +391,32 @@
             left if which == 0 else right,
         )
 
-    def forward(t):
+    def forward(t, parts=(0, 1)):
         block = rank_of(t)
-        for which in (0, 1):
-            block_copy(t, which, block, above).wait_recv()
+        place = block // 2
+        for which in parts:
+
+            @pl.when(place < table(t, limit[which]))
+            def _():
+                block_copy(t, which, block, above).wait_recv()
+
             for going, to in ((0, above), (1, below)):
-                entry = table(t, follow[going, which])
-
-                @pl.when(entry > 0)
+
+                @pl.when(place < table(t, next_limit[going, which]))
                 def _():
+                    entry = table(t, follow[going, which])
                     block_copy(entry, which, block, to).start()
 
-            x_copy(t, block, 1 - which).start()
+            @pl.when(block < rank)
+            def _():
+                x_copy(t, block, 1 - which).start()
+
 
     def arrived(t, block):
-        x_copy(t, block, 0).wait_recv()
-        x_copy(t, block, 1).wait_recv()
+        @pl.when(block <= rank)
+        def _():
+            x_copy(t, block, 0).wait_recv()
+            x_copy(t, block, 1).wait_recv()
 
     to_left.wait_recv()
     start_own(1)
@@ -429,12 +463,13 @@
 
     def expand(blocks):
         parts = (pl.ds(0, half), second)
+        def shown(b, value):
+            return jnp.where(b <= rank, value.astype(F32), 0.0)
+
         piece = [
-            jnp.concatenate([kvz[b, at, :].astype(F32) for b in blocks], axis=0) for at in parts
+            jnp.concatenate([shown(b, kvz[b, at, :]) for b in blocks], axis=0) for at in parts
         ]
-        piece += [
-            jnp.concatenate([kvx[b, i].astype(F32) for b in blocks], axis=0) for i in (0, 1)
-        ]
+        piece += [jnp.concatenate([shown(b, kvx[b, i]) for b in blocks], axis=0) for i in (0, 1)]
         squares = piece[0] * piece[0]
         for i in range(1, CHIPS):
             squares = squares + piece[i] * piece[i]
@@ -450,7 +485,7 @@
         values = dot(normed, wv2[...]).astype(BF16)
         rotary = []
         for b in blocks:
-            packed = kvz[b, half : half + half // 2, :].astype(F32)
+            packed = shown(b, kvz[b, half : half + half // 2, :])
             hidden = jnp.where(b <= rank, 0.0, masked_score).astype(F32)
             spare = jnp.where(lane == 64, hidden, 0.0)
             rotary.append(jnp.where(lane < 64, packed, spare))
@@ -502,22 +537,26 @@
             pool_out[:, at] = (dot(pooled, mix[g]) * scale).astype(BF16)
 
     forward(jnp.int32(3))
+    forward(jnp.int32(4))
     arrived(0, rank)
     arrived(1, rank_of(jnp.int32(1)))
     expand([rank, rank_of(jnp.int32(1))])
     attend_heads((0, 1), True)
-    forward(jnp.int32(4))
+    forward(jnp.int32(5))
     attend_heads((2, 3), True)
 
     def visit(i, carry):
-        @pl.when(2 * i + 3 < total_events)
-        def _():
-            forward(2 * i + 3)
-
-        earlier = [rank_of(2 * i), rank_of(2 * i + 1)]
+        first, then = 2 * i + 4, 2 * i + 5
+        events = [table(i, [pair[n] for pair in pairs]) for n in (0, 1)]
+        earlier = [rank_of(t) for t in events]
         seen = jnp.logical_or(earlier[0] < rank, earlier[1] < rank)
-        arrived(2 * i, earlier[0])
-        arrived(2 * i + 1, earlier[1])
+
+        @pl.when(first < total_events)
+        def _():
+            forward(first)
+
+        arrived(events[0], earlier[0])
+        arrived(events[1], earlier[1])
 
         @pl.when(seen)
         def _():
@@ -525,9 +564,9 @@
             attend_heads((0, 1), False)
 
 
-        @pl.when(2 * i + 4 < total_events)
-        def _():
-            forward(2 * i + 4)
+        @pl.when(then < total_events)
+        def _():
+            forward(then)
 
 
         @pl.when(seen)
@@ -642,14 +681,19 @@
     for cp in (halo_copy, qn_copy, acc_copy, stat_copy):
         cp.wait_send()
 
-    def drain(t, carry):
-        block_copy(t, 0, 0, above).wait_send()
-        block_copy(t, 1, 0, above).wait_send()
-        x_copy(t, 0, 0).wait_send()
-        x_copy(t, 0, 1).wait_send()
-        return carry
-
-    lax.fori_loop(1, total_events, drain, 0)
+    for t in range(1, total_events):
+        for which in (0, 1):
+            held = lax.rem(z + shift[parent[which][t]] + ring, ring)
+
+            @pl.when(held < limit[which][t])
+            def _():
+                block_copy(t, which, 0, above).wait_send()
+
+        @pl.when(rank_of(t) < rank)
+        def _():
+            x_copy(t, 0, 0).wait_send()
+            x_copy(t, 0, 1).wait_send()
+
     for n in range(chunks):
         for i in range(4):
 

time: 80.6 us -> 75.1 us (0.932)
  the two profiles are of different devices: /device:TPU:1 before, /device:TPU:257 now
where the time goes in v3:
time: 75.1 us; the launch traced here: 74.9 us
  Pallas kernels  72.1 us (96%)
  local copies, waits for them, and re-layouts  2.2 us (3%)
    pallas_call x1, Pallas kernels, per_device(): pl.pallas_call(functools.partial(kernel, sp_size), out_shape=(jax.ShapeDt...  72.1 us
    unnamed x4, local copies, waits for them, and re-layouts  2.2 us

profile of v3, /device:TPU:257, one launch (start us, length us, event | category | flops | bytes accessed | tf_op | source)
XLA Modules:
  0.0 74.9 jit_solution(10405478115858719326)
XLA Ops:
  0.6 72.1 %shard_map.185 = (bf16[48,2048]{1,0:T(8,128)(2,1)}, f32[2,384]{1,0:T(2,128)}) custom-call(bf16[384,256]{1,0:T(8,128)(2,1)} %tokens.1, f32[1,2048]{1,0:T(1,128)} %bitcast.11, bf16[2048,128]{1,0:T(8,128)(2,1)} %w_pool_in.1, bf16[64,2048]{1,0:T(8,128)(2,1)} %bitcast.8, bf16[64,2048]{1,0:T(8,128)(2,1)} %bitcast.9, bf16[64,2048]{1,0:T(8,128)(2,1)} %bitcast.10, ...), custom_call_target="tpu_custom_call" | custom-call | tf_op jit(solution)/shard_map/pallas_call | solution.py:746
  72.7 0.0 copy-start
  72.7 1.6 %copy.22 = bf16[48,2048]{1,0:T(8,128)(2,1)} copy(bf16[48,2048]{1,0:T(8,128)(2,1)} %get-tuple-element.8) | data formatting | bytes 393216
  74.4 0.0 copy-done
  74.4 0.6 copy.23
Async XLA Ops:
  72.7 1.6 %copy-start = (f32[2,384]{1,0:T(2,128)S(1)}, f32[2,384]{1,0:T(2,128)}, u32[]{:S(2)}) copy-start(f32[2,384]{1,0:T(2,128)} %get-tuple-element.5) | copy-start | bytes 9220

commit v4 on v3

--- a/solution.py
+++ b/solution.py
@@ -48,22 +48,24 @@
                 if k == 0 or direction == going:
                     if k + 1 < far:
                         entry = at[(column, going, k + 1)]
-                    elif which == going:
+                    elif going == 0 or which == 1:
                         entry = at[(column, 2, far)]
                 entries.append(entry)
             follow[going, which] = entries
     shift = [k if direction == 1 else -k for _, direction, k in order]
     limit = ([], [])
-    parent = ([], [])
     for which in (0, 1):
         for column, direction, k in order:
             bound = (ring - k, far - 1 + which, far)[direction]
             limit[which].append(bound)
-            before = at[(column, direction if direction < 2 else which, k - 1)] if k > 1 else 0
-            parent[which].append(at[(column, 0, 0)] if k == 1 else before)
-    next_limit = {
-        key: [limit[key[1]][e] if e else 0 for e in entries] for key, entries in follow.items()
-    }
+    next_limit, next_least = {}, {}
+    for (going, which), entries in follow.items():
+        to_far = [e > 0 and order[e][1] == 2 and which == 1 for e in entries]
+        next_limit[going, which] = [
+            (far - 1 if f and going == 0 else limit[which][e]) if e else 0
+            for e, f in zip(entries, to_far)
+        ]
+        next_least[going, which] = [far - 1 if f and going == 1 else 0 for f in to_far]
     when = {e: t for t, e in timed}
     pairs = []
     for above in (False, True):
@@ -71,12 +73,12 @@
         pairs += list(zip(group[::2], group[1::2]))
     pairs.sort(key=lambda pair: when[pair[1]])
     pairs = [[at[e] for e in pair] for pair in pairs]
-    return order, follow, shift, at[(1, 0, 0)], limit, next_limit, parent, pairs
+    return order, follow, shift, at[(1, 0, 0)], limit, next_limit, next_least, pairs
 
 
 def table(index, entries):
     if isinstance(index, int):
-        return entries[index]
+        return jnp.int32(entries[index])
     out = jnp.int32(entries[0])
     for i, entry in enumerate(entries):
         if i > 0 and entry != entries[0]:
@@ -102,25 +104,30 @@
 def kernel(
     sp_size,
     tokens,
-    mix_gain,
+    mix_gain_in,
     w_pool_in,
     w_qlat,
     w_kvlat,
     w_krope,
-    q_gain,
-    kv_gain,
+    q_gain_in,
+    kv_gain_in,
     w_qc,
     w_qr,
     w_key,
     w_value,
     pool_mix,
-    pool_scale,
+    pool_scale_in,
     w_out_pool,
     w_out_attn,
     base_tab,
-    rank_tab,
+    rank_tab_in,
     out,
     logt,
+    mix_gain,
+    q_gain,
+    kv_gain,
+    pool_scale,
+    rank_tab,
     tok,
     wp,
     wl,
@@ -169,6 +176,8 @@
     sem_one_r,
     sem_rs_s,
     sem_rs_r,
+    sem_relay_s,
+    sem_ready,
 ):
     sp = lax.axis_index("sp")
     tp = lax.axis_index("tp")
@@ -177,7 +186,12 @@
     x, c = tp // 2, tp % 2
     rank = sp // count
     z, yh = rank // 2, rank % 2
-    order, follow, shift, y_event, limit, next_limit, parent, pairs = event_list(ring)
+    order, follow, shift, y_event, limit, next_limit, next_least, pairs = event_list(ring)
+
+    def goes(t, going, which, place):
+        least = table(t, next_least[going, which])
+        return jnp.logical_and(place >= least, place < table(t, next_limit[going, which]))
+
     total_events = len(order)
     rows = tokens.shape[0]
     half = rows // 2
@@ -196,7 +210,6 @@
     below = lax.rem(sp + sp_size - ring_step, sp_size)
     beside = sp + count * (1 - 2 * yh)
     halo_sp = lax.rem(sp + count * c, sp_size)
-    halo_greet = lax.rem(sp + sp_size + count * (2 * c - 1), sp_size)
 
     core64 = pl.multiple_of(64 * c, 64)
     wl_q, wl_kv = core64, pl.multiple_of(128 + 64 * c, 64)
@@ -221,12 +234,17 @@
         (w_krope, wl.at[pl.ds(320, 64)]),
         (base_tab, tab),
         (pool_mix.at[pl.ds(2 * x, 2)], mix),
+        (mix_gain_in, mix_gain),
+        (q_gain_in, q_gain),
+        (kv_gain_in, kv_gain),
+        (pool_scale_in, pool_scale),
+        (rank_tab_in, rank_tab),
     ]
     local = [pltpu.make_async_copy(s, d, sem_local.at[i]) for i, (s, d) in enumerate(local)]
     given = [
         remote(s, d(), sem_ws.at[i], sem_wr.at[i], sp, partner) for i, (s, d) in enumerate(shared)
     ]
-    for i in [9, 10, 11, 0, 1, 2, 12, 3, 4, 5, 6, 13, 7, 8]:
+    for i in [9, 14, 18, 12, 10, 11, 0, 1, 2, 15, 16, 17, 3, 4, 5, 6, 13, 7, 8]:
         local[i].start()
 
     barrier = pltpu.get_barrier_semaphore()
@@ -234,37 +252,86 @@
         pl.semaphore_signal(
             barrier, inc=1, device_id={"sp": sp, "tp": lax.rem(tp + i, PEERS)}, device_id_type=MESH
         )
-    for other_sp, other_tp in (
-        (beside, tp),
-        (above, tp),
-        (below, tp),
-        (halo_greet, partner),
-    ):
+    def greet(other_sp, other_tp):
         pl.semaphore_signal(
             barrier, inc=1, device_id={"sp": other_sp, "tp": other_tp}, device_id_type=MESH
         )
-    pl.semaphore_wait(barrier, PEERS - 1 + 4)
-
-    def token_copy(i):
-        chip = x + (2, 2, 1, 1, 3, 3, 0)[i]
-        core = (0, 1, 0, 1, 0, 1, 1 - c)[i]
-        start = pl.multiple_of(half * core, half) if i == 6 else half * core
+
+    def answer(which, other_sp, other_tp):
+        pl.semaphore_signal(
+            sem_ready.at[which],
+            inc=1,
+            device_id={"sp": other_sp, "tp": other_tp},
+            device_id_type=MESH,
+        )
+
+    last_place = z == ring - 1
+    sends_halo = jnp.logical_and(c == 1, rank < SPAN - 1)
+    takes_halo = jnp.logical_and(c == 0, rank > 0)
+    greet(beside, tp)
+
+    @pl.when(jnp.logical_not(last_place))
+    def _():
+        greet(above, tp)
+
+    @pl.when(z == 0)
+    def _():
+        greet(below, tp)
+
+    @pl.when(sends_halo)
+    def _():
+        greet(halo_sp, partner)
+
+    greeters = PEERS + jnp.where(z > 0, 1, 0) + jnp.where(last_place, 1, 0)
+    pl.semaphore_wait(barrier, greeters + jnp.where(takes_halo, 1, 0))
+
+    @pl.when(z > 0)
+    def _():
+        answer(0, below, tp)
+
+    @pl.when(last_place)
+    def _():
+        answer(1, above, tp)
+
+    @pl.when(takes_halo)
+    def _():
+        answer(2, lax.rem(sp + sp_size - count, sp_size), partner)
+
+    def token_copy(i, part):
+        chip, core = x + (1, 1, 3, 3)[i], i % 2
+        at = pl.ds(part * (half // 2), half // 2)
         return remote(
-            tokens.at[pl.ds(start, half)],
-            tok.at[tp],
-            sem_ts.at[i],
-            sem_tr.at[tp],
+            tokens.at[pl.ds(half * core + part * (half // 2), half // 2)],
+            tok.at[tp, at],
+            sem_ts.at[i, part],
+            sem_tr.at[tp, part],
             sp,
             tp_of(chip, core),
         )
 
-    token_copies = [token_copy(i) for i in range(7)]
-    for i in (2, 4, 3, 5, 0, 1, 6):
-        token_copies[i].start()
+    def token_wait(source, part):
+        piece = tok.at[source, pl.ds(part * (half // 2), half // 2)]
+        remote(piece, piece, sem_ts.at[0, 0], sem_tr.at[source, part], sp, partner).wait_recv()
+
+    def token_relay(source, part, index, to):
+        piece = tok.at[source, pl.ds(part * (half // 2), half // 2)]
+        return remote(piece, piece, sem_relay_s.at[index], sem_tr.at[source, part], sp, to)
+
+    token_copies = [token_copy(i, part) for part in (0, 1) for i in (0, 1)]
+    token_copies += [token_copy(i, part) for part in (1, 0) for i in (2, 3)]
+    token_copies = [token_copies[i] for i in (0, 4, 1, 5, 2, 6, 3, 7)]
+    token_copies.append(
+        remote(
+            tokens.at[pl.ds(other_half, half)], tok.at[tp], sem_one_s.at[4], sem_one_r.at[4], sp, partner
+        )
+    )
+    for cp in token_copies:
+        cp.start()
     for g in given:
         g.start()
 
     local[12].wait()
+    local[18].wait()
     lane = lax.broadcasted_iota(jnp.int32, (1, 128), 1)
     low_part = (lane % 64) < 32
     sign = jnp.where(low_part, -1.0, 1.0).astype(F32)
@@ -278,7 +345,15 @@
         swapped = jnp.where(low_part, pltpu.roll(v, 96, 1), pltpu.roll(v, 32, 1))
         return v * cosine + swapped * signed_sine
 
-    for i in (0, 1, 2, 9, 10, 11):
+    relayed = []
+    for i, core in ((0, c), (1, 1 - c)):
+        for chip, piece, onward in ((1, 1, left), (3, 0, right)):
+            source = tp_of(x + chip, core)
+            token_wait(source, piece)
+            relay = token_relay(source, piece, len(relayed), onward)
+            relay.start()
+            relayed.append(relay)
+    for i in (0, 1, 2, 9, 10, 11, 14, 15, 16, 17):
         local[i].wait()
     for i in (0, 1, 2):
         given[i].wait_recv()
@@ -288,9 +363,17 @@
         chip = x + jnp.where(hop == 2, 3, jnp.where(hop == 3, 2, hop))
         source = tp_of(chip, (c + j) % 2)
 
-        @pl.when(j > 0)
-        def _():
-            remote(tok.at[source], tok.at[source], sem_ts.at[0], sem_tr.at[source], sp, partner).wait_recv()
+        @pl.when(j == 1)
+        def _():
+            remote(tok.at[source], tok.at[source], sem_one_s.at[4], sem_one_r.at[4], sp, partner).wait_recv()
+
+        @pl.when(jnp.logical_or(jnp.logical_and(j >= 2, j < 4), j >= 6))
+        def _():
+            token_wait(source, 0)
+
+        @pl.when(j >= 4)
+        def _():
+            token_wait(source, 1)
 
         at = pl.ds(pl.multiple_of(source * width, width), width)
         raw = tok[source].astype(F32)
@@ -334,7 +417,7 @@
         for going, to in ((0, above), (1, below)):
             if follow[going, which][0]:
 
-                @pl.when(z < next_limit[going, which][0])
+                @pl.when(goes(0, going, which, z))
                 def _():
                     block_copy(follow[going, which][0], which, rank, to).start()
 
@@ -350,11 +433,20 @@
     ]
     q_from = [lax.rem(x + 1, CHIPS), lax.rem(x + 3, CHIPS), lax.rem(x + 2, CHIPS)]
     to_left.start()
+
+    @pl.when(jnp.logical_not(last_place))
+    def _():
+        pl.semaphore_wait(sem_ready.at[0], 1)
+
+    @pl.when(z == 0)
+    def _():
+        pl.semaphore_wait(sem_ready.at[1], 1)
+
     start_own(0)
+    for q_copy in q_copies:
+        q_copy.start()
     to_right.start()
     to_across.start()
-    for q_copy in q_copies:
-        q_copy.start()
     halo_copy = remote(
         pool_own.at[pl.ds(half - 16, 16)],
         halo,
@@ -363,7 +455,18 @@
         halo_sp,
         partner,
     )
-    halo_copy.start()
+
+    @pl.when(sends_halo)
+    def _():
+        pl.semaphore_wait(sem_ready.at[2], 1)
+
+    halo_goes = jnp.logical_or(c == 0, sends_halo)
+    halo_comes = jnp.logical_or(c == 1, takes_halo)
+
+    @pl.when(halo_goes)
+    def _():
+        halo_copy.start()
+
 
     for i in (3, 4, 5, 6):
         local[i].wait()
@@ -402,7 +505,7 @@
 
             for going, to in ((0, above), (1, below)):
 
-                @pl.when(place < table(t, next_limit[going, which]))
+                @pl.when(goes(t, going, which, place))
                 def _():
                     entry = table(t, follow[going, which])
                     block_copy(entry, which, block, to).start()
@@ -516,10 +619,13 @@
             acc[h] = acc[h] * factor + dot(expo, values_at[:, at])
 
     def pooling():
-        remote(halo, halo, sem_one_s.at[0], sem_one_r.at[0], sp, partner).wait_recv()
+        @pl.when(halo_comes)
+        def _():
+            remote(halo, halo, sem_one_s.at[0], sem_one_r.at[0], sp, partner).wait_recv()
+
         local[13].wait()
         before = halo[...].astype(F32)
-        before = jnp.where(jnp.logical_and(rank == 0, c == 0), 0.0, before)
+        before = jnp.where(halo_comes, before, 0.0)
         row = lax.broadcasted_iota(jnp.int32, (half, 128), 0) + (rank * rows + own_half)
         odd = x % 2
         for g in (0, 1):
@@ -579,7 +685,22 @@
 
         return carry
 
-    lax.fori_loop(1, total_events // 2, visit, 0)
+    def visit_last(i, carry):
+        events = [table(i, [pair[n] for pair in pairs]) for n in (0, 1)]
+        earlier = [rank_of(t) for t in events]
+        arrived(events[0], earlier[0])
+        arrived(events[1], earlier[1])
+
+        @pl.when(jnp.logical_or(earlier[0] < rank, earlier[1] < rank))
+        def _():
+            expand(earlier)
+            attend_heads((0, 1, 2, 3), False)
+
+        return carry
+
+    all_sent = (total_events - 4) // 2
+    lax.fori_loop(1, all_sent, visit, 0)
+    lax.fori_loop(all_sent, total_events // 2, visit_last, 0)
 
     acc_copy = remote(
         acc.at[:, pl.ds(other_half, half), :], acc_in, sem_one_s.at[2], sem_one_r.at[2], sp, partner
@@ -637,7 +758,7 @@
     def part_keep(n):
         at = pl.ds(n * chunk, chunk)
         return pltpu.make_async_copy(
-            part.at[pl.ds(own_at, quarter), at], rs.at[x, :, at], sem_local.at[14 + n]
+            part.at[pl.ds(own_at, quarter), at], rs.at[x, :, at], sem_local.at[19 + n]
         )
 
     for n in range(chunks):
@@ -675,19 +796,33 @@
 
     for cp in token_copies + given + q_copies:
         cp.wait_send()
+    for relay in relayed:
+        relay.wait_send()
     to_left.wait_send()
     to_right.wait_send()
     to_across.wait_send()
-    for cp in (halo_copy, qn_copy, acc_copy, stat_copy):
+    for cp in (qn_copy, acc_copy, stat_copy):
         cp.wait_send()
 
+    @pl.when(halo_goes)
+    def _():
+        halo_copy.wait_send()
+
+
+    for which in (0, 1):
+        block_copy(y_event, which, 0, beside).wait_send()
+    for t in range(total_events):
+        held = rank_of(t) // 2
+        for which in (0, 1):
+            for going, to in ((0, above), (1, below)):
+                entry = follow[going, which][t]
+                if entry:
+
+                    @pl.when(goes(t, going, which, held))
+                    def _():
+                        block_copy(entry, which, 0, to).wait_send()
+
     for t in range(1, total_events):
-        for which in (0, 1):
-            held = lax.rem(z + shift[parent[which][t]] + ring, ring)
-
-            @pl.when(held < limit[which][t])
-            def _():
-                block_copy(t, which, 0, above).wait_send()
 
         @pl.when(rank_of(t) < rank)
         def _():
@@ -749,28 +884,14 @@
             jax.ShapeDtypeStruct((rows // PEERS, columns), BF16),
             jax.ShapeDtypeStruct((2, rows), F32),
         ),
-        in_specs=[
-            anywhere,
-            near,
-            anywhere,
-            anywhere,
-            anywhere,
-            anywhere,
-            near,
-            near,
-            anywhere,
-            anywhere,
-            anywhere,
-            anywhere,
-            anywhere,
-            near,
-            anywhere,
-            anywhere,
-            anywhere,
-            near,
-        ],
+        in_specs=[anywhere] * 18,
         out_specs=(near, near),
         scratch_shapes=[
+            vmem((1, features), F32),
+            vmem((1, 512), F32),
+            vmem((1, 512), F32),
+            vmem((1, 1024), F32),
+            vmem((2, SPAN, 128), F32),
             vmem((PEERS, half, width), BF16),
             vmem((2, features, 128), BF16),
             vmem((384, features), BF16),
@@ -804,21 +925,23 @@
             vmem((4, half, 128), F32),
             vmem((half, columns), BF16),
             vmem((CHIPS, rows // PEERS, columns), BF16),
-            dma(14 + chunks),
+            dma(19 + chunks),
             dma(9),
             dma(9),
-            dma(7),
-            dma(PEERS),
+            dma(4, 2),
+            dma(PEERS, 2),
             dma(total_events, 2),
             dma(total_events, 2),
             dma(total_events, 2),
             dma(total_events, 2),
             dma(3),
             dma(3),
-            dma(4),
-            dma(4),
+            dma(5),
+            dma(5),
             dma(4, chunks),
             dma(CHIPS, chunks),
+            dma(4),
+            pltpu.SemaphoreType.REGULAR((3,)),
         ],
         compiler_params=pltpu.CompilerParams(
             collective_id=0, has_side_effects=True, vmem_limit_bytes=56 * 1024 * 1024

time: 75.1 us -> 71 us (0.945)
  the two profiles are of different devices: /device:TPU:257 before, /device:TPU:449 now
where the time goes in v4:
time: 71 us; the launch traced here: 70.1 us
  Pallas kernels  67.2 us (95%)
  local copies, waits for them, and re-layouts  2.2 us (3%)
    pallas_call x1, Pallas kernels, per_device(): pl.pallas_call(functools.partial(kernel, sp_size), out_shape=(jax.ShapeDt...  67.2 us
    unnamed x4, local copies, waits for them, and re-layouts  2.2 us

profile of v4, /device:TPU:449, one launch (start us, length us, event | category | flops | bytes accessed | tf_op | source)
XLA Modules:
  0.0 70.1 jit_solution(17710089543495455639)
XLA Ops:
  0.6 67.2 %shard_map.185 = (bf16[48,2048]{1,0:T(8,128)(2,1)}, f32[2,384]{1,0:T(2,128)}) custom-call(bf16[384,256]{1,0:T(8,128)(2,1)} %tokens.1, f32[1,2048]{1,0:T(1,128)} %bitcast.11, bf16[2048,128]{1,0:T(8,128)(2,1)} %w_pool_in.1, bf16[64,2048]{1,0:T(8,128)(2,1)} %bitcast.8, bf16[64,2048]{1,0:T(8,128)(2,1)} %bitcast.9, bf16[64,2048]{1,0:T(8,128)(2,1)} %bitcast.10, ...), custom_call_target="tpu_custom_call" | custom-call | tf_op jit(solution)/shard_map/pallas_call | solution.py:881
  67.9 0.0 copy-start
  67.9 1.6 %copy.22 = bf16[48,2048]{1,0:T(8,128)(2,1)} copy(bf16[48,2048]{1,0:T(8,128)(2,1)} %get-tuple-element.8) | data formatting | bytes 393216
  69.5 0.0 copy-done
  69.5 0.6 copy.23
Async XLA Ops:
  67.9 1.6 %copy-start = (f32[2,384]{1,0:T(2,128)S(1)}, f32[2,384]{1,0:T(2,128)}, u32[]{:S(2)}) copy-start(f32[2,384]{1,0:T(2,128)} %get-tuple-element.5) | copy-start | bytes 9220

commit v5 on v4

--- a/solution.py
+++ b/solution.py
@@ -35,7 +35,8 @@
         timed.append((first, (column, 0, 0)))
         for k in range(1, far):
             timed.append((first + pace * k, (column, 0, k)))
-            timed.append((first + pace * k + 0.1, (column, 1, k)))
+            late = 5.0 if column == 1 and k == far - 1 else 0.1
+            timed.append((first + pace * k + late, (column, 1, k)))
         timed.append((first + pace * far, (column, 2, far)))
     order = [e for _, e in sorted(timed)]
     at = {e: i for i, e in enumerate(order)}
@@ -121,7 +122,7 @@
     w_out_attn,
     base_tab,
     rank_tab_in,
-    out,
+    rs,
     logt,
     mix_gain,
     q_gain,
@@ -160,7 +161,6 @@
     sum_at,
     acc_in,
     part,
-    rs,
     sem_local,
     sem_ws,
     sem_wr,
@@ -524,8 +524,8 @@
     to_left.wait_recv()
     start_own(1)
 
-    forward(jnp.int32(1))
-    forward(jnp.int32(2))
+    forward(jnp.int32(1), (0,))
+    forward(jnp.int32(2), (0,))
     for i, piece in enumerate(q_from):
         remote(
             qbuf.at[piece], qbuf.at[piece], sem_qs.at[i], sem_qr.at[i], sp, left
@@ -547,6 +547,8 @@
         partner,
     )
     qn_copy.start()
+    forward(jnp.int32(1), (1,))
+    forward(jnp.int32(2), (1,))
     qn_other = qn.at[pl.ds(other_half, half)]
     remote(qn_other, qn_other, sem_one_s.at[1], sem_one_r.at[1], sp, partner).wait_recv()
     normed = qn[...]
@@ -642,6 +644,7 @@
             scale = pool_scale[:, pl.ds(pl.multiple_of(256 * x + 128 * g, 128), 128)]
             pool_out[:, at] = (dot(pooled, mix[g]) * scale).astype(BF16)
 
+    pooling()
     forward(jnp.int32(3))
     forward(jnp.int32(4))
     arrived(0, rank)
@@ -678,10 +681,6 @@
         @pl.when(seen)
         def _():
             attend_heads((2, 3), False)
-
-        @pl.when(i == 1)
-        def _():
-            pooling()
 
         return carry
 
@@ -787,13 +786,6 @@
                 ref = rs.at[chip, :, pl.ds(n * chunk, chunk)]
                 remote(ref, ref, sem_rs_s.at[0, n], sem_rs_r.at[chip, n], sp, partner).wait_recv()
 
-        out[:, at] = (
-            rs[0, :, at].astype(F32)
-            + rs[1, :, at].astype(F32)
-            + rs[2, :, at].astype(F32)
-            + rs[3, :, at].astype(F32)
-        ).astype(BF16)
-
     for cp in token_copies + given + q_copies:
         cp.wait_send()
     for relay in relayed:
@@ -881,11 +873,11 @@
     out, logt = pl.pallas_call(
         functools.partial(kernel, sp_size),
         out_shape=(
-            jax.ShapeDtypeStruct((rows // PEERS, columns), BF16),
-            jax.ShapeDtypeStruct((2, rows), F32),
+            pltpu.VMEM((CHIPS, rows // PEERS, columns), BF16),
+            pltpu.VMEM((2, rows), F32),
         ),
         in_specs=[anywhere] * 18,
-        out_specs=(near, near),
+        out_specs=(anywhere, near),
         scratch_shapes=[
             vmem((1, features), F32),
             vmem((1, 512), F32),
@@ -924,7 +916,6 @@
             vmem((4, rows, 128), F32),
             vmem((4, half, 128), F32),
             vmem((half, columns), BF16),
-            vmem((CHIPS, rows // PEERS, columns), BF16),
             dma(19 + chunks),
             dma(9),
             dma(9),
@@ -966,7 +957,8 @@
         jnp.asarray(base_tab),
         jnp.asarray(rank_tab),
     )
-    return out, logt.T
+    wide = [out[i].astype(F32) for i in range(CHIPS)]
+    return (wide[0] + wide[1] + wide[2] + wide[3]).astype(BF16), logt.T
 
 
 def solution(mesh):

time: 71 us -> 68 us (0.958); the launches traced: 70.1 us -> 67.9 us
  local copies, waits for them, and re-layouts: 2.2 us -> 0.58 us
  Pallas kernels: 67.2 us -> 65.9 us
  other arithmetic: 0 us -> 0.78 us
    unnamed x4 -> x1, local copies, waits for them, and re-layouts: 2.2 us -> 0.58 us
    pallas_call x1, Pallas kernels: 67.2 us -> 65.9 us  [per_device(): pl.pallas_call(functools.partial(kernel, sp_size), out_shape=(pltpu.VMEM(...]
    add x0 -> x1, other arithmetic: none -> 0.78 us  [per_device(): return ((wide[0] + wide[1] + wide[2] + wide[3]).astype(BF16), logt.T)]
where the time goes in v5:
time: 68 us; the launch traced here: 67.9 us
  Pallas kernels  65.9 us (97%)
  other arithmetic  0.78 us (1%)
    pallas_call x1, Pallas kernels, per_device(): pl.pallas_call(functools.partial(kernel, sp_size), out_shape=(pltpu.VMEM(...  65.9 us

profile of v5, /device:TPU:449, one launch (start us, length us, event | category | flops | bytes accessed | tf_op | source)
XLA Modules:
  0.0 67.9 jit_solution(18204698869763156999)
XLA Ops:
  0.6 65.9 %shard_map.185 = (bf16[4,48,2048]{2,1,0:T(8,128)(2,1)S(1)}, f32[2,384]{1,0:T(2,128)S(1)}) custom-call(bf16[384,256]{1,0:T(8,128)(2,1)} %tokens.1, f32[1,2048]{1,0:T(1,128)} %bitcast.14, bf16[2048,128]{1,0:T(8,128)(2,1)} %w_pool_in.1, bf16[64,2048]{1,0:T(8,128)(2,1)} %bitcast.11, bf16[64,2048]{1,0:T(8,128)(2,1)} %bitcast.12, bf16[64,2048]{1,0:T(8,128)(2,1)} %bitcast.13, ...), custom_call_target="tpu_custom_call" | custom-call | tf_op jit(solution)/shard_map/pallas_call | solution.py:873
  66.5 0.8 %fusion = bf16[48,2048]{1,0:T(8,128)(2,1)} fusion(bf16[4,48,2048]{2,1,0:T(8,128)(2,1)S(1)} %get-tuple-element.4), kind=kLoop, calls=%fused_computation.1 | loop fusion | flops 786432 | bytes 983040 | tf_op jit(solution)/shard_map/add | solution.py:961
  67.3 0.6 copy.21

commit v6 on v5

--- a/solution.py
+++ b/solution.py
@@ -268,7 +268,9 @@
     last_place = z == ring - 1
     sends_halo = jnp.logical_and(c == 1, rank < SPAN - 1)
     takes_halo = jnp.logical_and(c == 0, rank > 0)
-    greet(beside, tp)
+    @pl.when(yh == 0)
+    def _():
+        greet(beside, tp)
 
     @pl.when(jnp.logical_not(last_place))
     def _():
@@ -278,12 +280,23 @@
     def _():
         greet(below, tp)
 
-    @pl.when(sends_halo)
+    before_sp = lax.rem(sp + sp_size - count, sp_size)
+
+    @pl.when(jnp.logical_and(c == 1, yh == 0))
     def _():
         greet(halo_sp, partner)
 
-    greeters = PEERS + jnp.where(z > 0, 1, 0) + jnp.where(last_place, 1, 0)
-    pl.semaphore_wait(barrier, greeters + jnp.where(takes_halo, 1, 0))
+    @pl.when(jnp.logical_and(takes_halo, yh == 0))
+    def _():
+        greet(before_sp, partner)
+
+    greeters = PEERS - 1 + yh + jnp.where(z > 0, 1, 0) + jnp.where(last_place, 1, 0)
+    of_halo = jnp.logical_and(yh == 1, jnp.logical_or(takes_halo, sends_halo))
+    pl.semaphore_wait(barrier, greeters + jnp.where(of_halo, 1, 0))
+
+    @pl.when(yh == 1)
+    def _():
+        answer(3, beside, tp)
 
     @pl.when(z > 0)
     def _():
@@ -293,9 +306,9 @@
     def _():
         answer(1, above, tp)
 
-    @pl.when(takes_halo)
-    def _():
-        answer(2, lax.rem(sp + sp_size - count, sp_size), partner)
+    @pl.when(jnp.logical_and(takes_halo, yh == 1))
+    def _():
+        answer(2, before_sp, partner)
 
     def token_copy(i, part):
         chip, core = x + (1, 1, 3, 3)[i], i % 2
@@ -441,6 +454,10 @@
     @pl.when(z == 0)
     def _():
         pl.semaphore_wait(sem_ready.at[1], 1)
+
+    @pl.when(yh == 0)
+    def _():
+        pl.semaphore_wait(sem_ready.at[3], 1)
 
     start_own(0)
     for q_copy in q_copies:
@@ -456,7 +473,7 @@
         partner,
     )
 
-    @pl.when(sends_halo)
+    @pl.when(jnp.logical_and(c == 1, yh == 0))
     def _():
         pl.semaphore_wait(sem_ready.at[2], 1)
 
@@ -932,7 +949,7 @@
             dma(4, chunks),
             dma(CHIPS, chunks),
             dma(4),
-            pltpu.SemaphoreType.REGULAR((3,)),
+            pltpu.SemaphoreType.REGULAR((4,)),
         ],
         compiler_params=pltpu.CompilerParams(
             collective_id=0, has_side_effects=True, vmem_limit_bytes=56 * 1024 * 1024

time: 68 us -> 67.2 us (0.988)
  Pallas kernels: 65.9 us -> 65.1 us
    pallas_call x1, Pallas kernels: 65.9 us -> 65.1 us  [per_device(): pl.pallas_call(functools.partial(kernel, sp_size), out_shape=(pltpu.VMEM(...]
where the time goes in v6:
time: 67.2 us; the launch traced here: 67.1 us
  Pallas kernels  65.1 us (97%)
  other arithmetic  0.78 us (1%)
    pallas_call x1, Pallas kernels, per_device(): pl.pallas_call(functools.partial(kernel, sp_size), out_shape=(pltpu.VMEM(...  65.1 us

profile of v6, /device:TPU:449, one launch (start us, length us, event | category | flops | bytes accessed | tf_op | source)
XLA Modules:
  0.0 67.1 jit_solution(17342782696052179572)
XLA Ops:
  0.6 65.1 %shard_map.185 = (bf16[4,48,2048]{2,1,0:T(8,128)(2,1)S(1)}, f32[2,384]{1,0:T(2,128)S(1)}) custom-call(bf16[384,256]{1,0:T(8,128)(2,1)} %tokens.1, f32[1,2048]{1,0:T(1,128)} %bitcast.14, bf16[2048,128]{1,0:T(8,128)(2,1)} %w_pool_in.1, bf16[64,2048]{1,0:T(8,128)(2,1)} %bitcast.11, bf16[64,2048]{1,0:T(8,128)(2,1)} %bitcast.12, bf16[64,2048]{1,0:T(8,128)(2,1)} %bitcast.13, ...), custom_call_target="tpu_custom_call" | custom-call | tf_op jit(solution)/shard_map/pallas_call | solution.py:890
  65.8 0.8 %fusion = bf16[48,2048]{1,0:T(8,128)(2,1)} fusion(bf16[4,48,2048]{2,1,0:T(8,128)(2,1)S(1)} %get-tuple-element.4), kind=kLoop, calls=%fused_computation.1 | loop fusion | flops 786432 | bytes 983040 | tf_op jit(solution)/shard_map/add | solution.py:978
  66.5 0.6 copy.21
